TPU v7x, 512 devices: a whole 4x8x8 slice. The times are simulated.
512 devices in a mesh: sp: 64 (over z, y), tp: 4 (over x), dp: 2 (over core).
Axes of the slice: x: 4, y: 8, z: 8, core: 2. Of those that a mesh axis runs over, the one named last changes fastest.
Arguments:
- latent: bfloat16 [2, 8192, 2048], P('dp', ('sp', 'tp')), may hold values from -10 to 10
- condition: bfloat16 [2, 2048], P('dp'), may hold values from -6 to 6
- context: bfloat16 [2, 512, 2048], P('dp', 'sp'), may hold values from -6 to 6
- context_source: bfloat16 [2048], replicated, may hold values from -6 to 6
- mod_weight: bfloat16 [3, 2048, 2048], P(None, 'sp', 'tp'), may hold values from -0.125 to 0.125
- norm_gain: bfloat16 [2048], replicated, may hold values from 0.099609375 to 1.8984375
- w_x: bfloat16 [2048, 2048], P('dp', 'tp'), may hold values from -0.125 to 0.125
- w_b: bfloat16 [2048, 512], P('dp', 'tp'), may hold values from -0.125 to 0.125
- w_c: bfloat16 [2048, 512], P('dp', 'tp'), may hold values from -0.125 to 0.125
- w_z: bfloat16 [2048, 2048], P('dp', 'tp'), may hold values from -0.125 to 0.125
- w_dt: bfloat16 [2, 2048, 32], P(None, 'dp', 'tp'), may hold values from -0.125 to 0.125
- conv_x: bfloat16 [3, 2048], P(None, 'tp'), may hold values from -3.5 to 3.5
- conv_b: bfloat16 [3, 512], P(None, 'tp'), may hold values from -3.5 to 3.5
- conv_c: bfloat16 [3, 512], P(None, 'tp'), may hold values from -3.5 to 3.5
- decay_rate: float32 [2, 32], P(None, 'tp'), may hold values from 0 to 1, as said below
- out_gain: bfloat16 [2048], P('tp'), may hold values from 0.099609375 to 1.8984375
- w_out: bfloat16 [2048, 2048], P(('tp', 'dp')), may hold values from -0.125 to 0.125
Outputs:
- update: bfloat16 [2, 8192, 2048], P('dp', ('sp', 'tp'))
Inputs may be any that keep to these rules, and one draw needn't show every extreme that they name: `decay_rate`: positive rates.
All inputs are finite; a program needn't handle non-finite values.
Results may differ from a plain program's by a relative error of at most 0.014.
Values may be sent and summed in bfloat16 or wider, within the bound.
A program may use at most 128 MiB of HBM per device.

v0:
```python
import functools

import jax
import jax.numpy as jnp
from jax import lax
from jax.sharding import Mesh
from jax.sharding import PartitionSpec as P

STATE = 128
BLOCK = 128
SP = ("sp_0", "sp_1")
SP_TP = ("sp_0", "sp_1", "tp")


EPSILON = 1e-06


def over_axes(x, axes):
    return functools.reduce(lax.psum, axes, x)


def laid_out(tiles, dim):
    tiles = jnp.moveaxis(tiles, 0, dim)
    dims = tiles.shape
    return tiles.reshape(*dims[:dim], dims[dim] * dims[dim + 1], *dims[dim + 2 :])


def sent_to_all(x, axis):
    peers = lax.axis_size(axis)
    return lax.all_to_all(jnp.broadcast_to(x[None], (peers, *x.shape)), axis, 0, 0, tiled=True)


def gather_directly(x, axis, dim):
    return laid_out(sent_to_all(x, axis), dim)


def sent_together(arrays, axis, dim, along):
    ends, at = ([], 0)
    for a in arrays[:-1]:
        at += a.shape[along]
        ends.append(at)
    both = jnp.concatenate(arrays, axis=along)
    return tuple(jnp.split(lax.all_gather(both, axis, axis=dim, tiled=True), ends, axis=along))


def with_halo(x, sides, width):
    for axis, dim in sides:
        peers, length = (lax.axis_size(axis), x.shape[dim])
        up = [(i, (i + 1) % peers) for i in range(peers - 1)]
        down = [(j, i) for i, j in up]
        last = lax.slice_in_dim(x, length - width, length, axis=dim)
        leading = lax.slice_in_dim(x, 0, width, axis=dim)
        before = lax.ppermute(last, axis, up)
        after = lax.ppermute(leading, axis, down)
        x = jnp.concatenate([before, x, after], axis=dim)
    return x


def neutral_like(x, identity):
    return jax.tree.map(
        lambda a, e: jnp.broadcast_to(jnp.asarray(e, a.dtype), a.shape), x, identity
    )


def entering_2(x, axes, combine, identity, reverse):
    before = start = neutral_like(x, identity)
    total = x
    for axis in reversed(axes):
        peers, place = (lax.axis_size(axis), lax.axis_index(axis))
        pieces = jax.tree.map(
            lambda part, kind: lax.all_gather(part.astype(kind), axis),
            total,
            (jnp.bfloat16, jnp.bfloat16),
        )
        inside, total = (start, start)
        for k in reversed(range(peers)) if reverse else range(peers):
            passed = k > place if reverse else k < place
            total = combine(
                total, jax.tree.map(lambda part, own: part[k].astype(own.dtype), pieces, x)
            )
            inside = jax.tree.map(lambda new, old: jnp.where(passed, new, old), total, inside)
        before = combine(inside, before)
    return before


def split_up(x, dim, peers):
    before, after = (x.shape[:dim], x.shape[dim + 1 :])
    return jnp.moveaxis(x.reshape(*before, peers, -1, *after), dim, 0)


def sum_at_owner(x, axis, dim):
    peers = lax.axis_size(axis)
    tiles = lax.all_to_all(split_up(x, dim, peers), axis, 0, 0, tiled=True)
    return jnp.sum(tiles.astype(jnp.float32), axis=0)


def rounded(values):
    return lax.optimization_barrier(values.astype(jnp.bfloat16)).astype(jnp.float32)


def modulated(source, gain_vec, shift_vec, scale_vec):
    values = source.astype(jnp.float32)
    normed = values * lax.rsqrt(jnp.mean(values * values, axis=-1, keepdims=True) + EPSILON)
    return (normed * gain_vec.astype(jnp.float32) * (1.0 + scale_vec) + shift_vec).astype(
        jnp.bfloat16
    )


def convolved(padded, weight, total_rows):
    wide_vals = padded.astype(jnp.float32)
    tap_weights = weight.astype(jnp.float32)
    summed = jnp.zeros((total_rows, wide_vals.shape[1]), jnp.float32)
    for offset in range(weight.shape[0]):
        summed = summed + wide_vals[offset : offset + total_rows] * tap_weights[offset]
    return jax.nn.silu(summed).astype(jnp.bfloat16)


def final_state(x_vals, b_vals, step_size, rate_head, groups):
    total_rows, head_count = step_size.shape
    per_group = head_count // groups
    moved_x = rounded(
        x_vals.reshape(total_rows, head_count, -1).astype(jnp.float32) * step_size[:, :, None]
    )
    running = jnp.cumsum(-rate_head * step_size, axis=0)
    weight = jnp.exp(running[-1:] - running)
    scaled = (moved_x * weight[:, :, None]).reshape(total_rows, groups, per_group, -1)
    b_wide = b_vals.reshape(total_rows, groups, -1).astype(jnp.float32)
    ctx_state = jnp.einsum("sgn,sghp->ghpn", b_wide, scaled)
    return (ctx_state, running[-1].reshape(groups, per_group))


def combine_states(earlier, later_part):
    return (
        earlier[0] + later_part[0],
        earlier[1] * jnp.exp(later_part[0])[:, :, None, None] + later_part[1],
    )


def direction_terms(x_vals, b_vals, c_vals, step_size, rate_head, groups):
    total_rows, head_count = step_size.shape
    per_group = head_count // groups
    blocks = total_rows // BLOCK
    moved_x = (
        x_vals.reshape(total_rows, head_count, -1).astype(jnp.float32) * step_size[:, :, None]
    ).astype(jnp.bfloat16)
    head_dim = moved_x.shape[2]
    x_blocks = moved_x.reshape(blocks, BLOCK, groups, per_group, head_dim)
    b_blocks = b_vals.reshape(blocks, BLOCK, groups, -1)
    c_blocks = c_vals.reshape(blocks, BLOCK, groups, -1)
    running = jnp.cumsum((-rate_head * step_size).reshape(blocks, BLOCK, head_count), axis=1)
    across = jnp.swapaxes(running, 1, 2)
    spread = across[:, :, :, None] - across[:, :, None, :]
    lower_part = lax.broadcasted_iota(jnp.int32, (BLOCK, BLOCK), 0) >= lax.broadcasted_iota(
        jnp.int32, (BLOCK, BLOCK), 1
    )
    decay_mask = jnp.where(lower_part, jnp.exp(jnp.minimum(spread, 0.0)), 0.0).reshape(
        blocks, groups, per_group, BLOCK, BLOCK
    )
    scores = jnp.einsum("clgn,csgn->cgls", c_blocks, b_blocks, preferred_element_type=jnp.float32)
    weights = (scores[:, :, None] * decay_mask).astype(jnp.bfloat16)
    inside = jnp.einsum("cghls,csghp->clghp", weights, x_blocks, preferred_element_type=jnp.float32)
    to_end = jnp.exp(running[:, -1:, :] - running).reshape(blocks, BLOCK, groups, per_group, 1)
    x_end = (x_blocks.astype(jnp.float32) * to_end).astype(jnp.bfloat16)
    fresh_state = jnp.einsum(
        "csgn,csghp->cghpn", b_blocks, x_end, preferred_element_type=jnp.float32
    )
    totals = running[:, -1, :].reshape(blocks, groups, per_group)

    def advance(carried_in, inputs):
        return (carried_in * jnp.exp(inputs[1])[:, :, None, None] + inputs[0], carried_in)

    ending, before = lax.scan(
        advance, jnp.zeros(fresh_state.shape[1:], jnp.float32), (fresh_state, totals)
    )
    return (inside, before, ending, totals, running, c_blocks)


def direction_output(terms, incoming):
    inside, before, ending, totals, running, c_blocks = terms
    blocks, length, groups, per_group, head_dim = inside.shape
    offset_sum = jnp.cumsum(totals, axis=0) - totals
    entering = before + jnp.exp(offset_sum)[:, :, :, None, None] * incoming[None]
    carried = jnp.einsum(
        "clgn,cghpn->clghp",
        c_blocks,
        entering.astype(jnp.bfloat16),
        preferred_element_type=jnp.float32,
    )
    growth = jnp.exp(running).reshape(blocks, length, groups, per_group, 1)
    return (inside + growth * carried).reshape(blocks * length, -1)


def shards(
    latent,
    condition,
    context,
    context_source,
    mod_weight,
    norm_gain,
    w_x,
    w_b,
    w_c,
    w_z,
    w_dt,
    conv_x,
    conv_b,
    conv_c,
    decay_rate,
    out_gain,
    w_out,
):
    row_count = mod_weight.shape[1]
    activations = jnp.stack(
        [
            jax.nn.silu(condition[0].astype(jnp.float32)),
            jax.nn.silu(context_source.astype(jnp.float32)),
        ]
    ).astype(jnp.bfloat16)
    own_rows = lax.dynamic_slice_in_dim(activations, lax.axis_index(SP) * row_count, row_count, 1)
    partial_value = jnp.einsum(
        "ar,krc->kac", own_rows, mod_weight, preferred_element_type=jnp.float32
    )
    summed = over_axes(partial_value, SP)
    mod_vectors = gather_directly(summed, "tp", 2)
    full_x, full_b, full_c, full_z, full_fwd, full_bwd, full_out = (
        *sent_together((w_x, w_b, w_c, w_z, w_dt[0], w_dt[1]), "dp", 0, 1),
        lax.all_gather(w_out, "dp", axis=0, tiled=True),
    )
    inner_cols = full_x.shape[1]
    gn_cols = full_b.shape[1]
    head_count = full_fwd.shape[1]
    groups = gn_cols // STATE
    mixed_cols = inner_cols + gn_cols
    reach_rows = conv_x.shape[0] // 2
    rate_fwd = decay_rate[0]
    rate_bwd = decay_rate[1]
    all_weights = jnp.concatenate([full_x, full_b, full_c, full_fwd, full_bwd, full_z], axis=1)
    ctx_weight = jnp.concatenate([full_x, full_b, full_fwd, full_bwd], axis=1)
    taps_all = jnp.concatenate([conv_x, conv_b, conv_c], axis=1)
    ctx_taps = jnp.concatenate([conv_x, conv_b], axis=1)
    ctx_rows = modulated(context[0], norm_gain, mod_vectors[0, 1], mod_vectors[1, 1])
    own_features = jnp.dot(ctx_rows, ctx_weight, preferred_element_type=jnp.float32).astype(
        jnp.bfloat16
    )
    features = gather_directly(own_features, SP, 0)
    total_rows = features.shape[0]
    padded = jnp.pad(features[:, :mixed_cols], ((reach_rows, reach_rows), (0, 0)))
    smoothed = convolved(padded, ctx_taps, total_rows)
    step_size = jax.nn.softplus(features[:, mixed_cols:].astype(jnp.float32))
    ctx_x = smoothed[:, :inner_cols]
    ctx_b = smoothed[:, inner_cols:]
    state_fwd, _ = final_state(ctx_x, ctx_b, step_size[:, :head_count], rate_fwd, groups)
    state_bwd, _ = final_state(
        jnp.flip(ctx_x, 0),
        jnp.flip(ctx_b, 0),
        jnp.flip(step_size[:, head_count:], 0),
        rate_bwd,
        groups,
    )
    latent_rows = modulated(latent[0], norm_gain, mod_vectors[0, 0], mod_vectors[1, 0])
    features = jnp.dot(
        gather_directly(latent_rows, "tp", 0), all_weights, preferred_element_type=jnp.float32
    ).astype(jnp.bfloat16)
    total_rows = features.shape[0]
    padded = with_halo(features[:, : mixed_cols + gn_cols], ((SP, 0),), reach_rows)
    smoothed = convolved(padded, taps_all, total_rows)
    x_vals = smoothed[:, :inner_cols]
    b_vals = smoothed[:, inner_cols:mixed_cols]
    c_vals = smoothed[:, mixed_cols:]
    base_col = mixed_cols + gn_cols
    step_size = jax.nn.softplus(
        features[:, base_col : base_col + 2 * head_count].astype(jnp.float32)
    )
    gate_in = features[:, base_col + 2 * head_count :]
    forward_terms = direction_terms(
        x_vals, b_vals, c_vals, step_size[:, :head_count], rate_fwd, groups
    )
    backward_terms = direction_terms(
        jnp.flip(x_vals, 0),
        jnp.flip(b_vals, 0),
        jnp.flip(c_vals, 0),
        jnp.flip(step_size[:, head_count:], 0),
        rate_bwd,
        groups,
    )
    fwd_total = jnp.sum(forward_terms[3], axis=0)
    bwd_total = jnp.sum(backward_terms[3], axis=0)
    empty = (jnp.zeros_like(fwd_total), jnp.zeros_like(forward_terms[2]))
    prefix_decay, prefix_state = entering_2(
        (fwd_total, forward_terms[2]), SP, combine_states, empty, False
    )
    suffix_decay, suffix_state = entering_2(
        (bwd_total, backward_terms[2]), SP, combine_states, empty, True
    )
    out_fwd = direction_output(
        forward_terms, prefix_state + jnp.exp(prefix_decay)[:, :, None, None] * state_fwd
    )
    out_bwd = jnp.flip(
        direction_output(
            backward_terms, suffix_state + jnp.exp(suffix_decay)[:, :, None, None] * state_bwd
        ),
        0,
    )
    gated = (out_fwd + out_bwd) * jax.nn.silu(gate_in.astype(jnp.float32))
    grouped = gated.reshape(total_rows, groups, -1)
    normed = (
        grouped
        * lax.rsqrt(jnp.mean(grouped * grouped, axis=-1, keepdims=True) + EPSILON)
        * out_gain.reshape(groups, -1).astype(jnp.float32)
    )
    normed_out = normed.reshape(total_rows, -1).astype(jnp.bfloat16)
    mixed = sum_at_owner(
        jnp.dot(normed_out, full_out, preferred_element_type=jnp.float32).astype(jnp.bfloat16),
        "tp",
        0,
    )
    return (mod_vectors[2, 0] * mixed).astype(jnp.bfloat16)[None]


def solution(mesh):
    torus = Mesh(
        mesh.devices.reshape(8, 8, mesh.shape["tp"], mesh.shape["dp"]), ("sp_0", "sp_1", "tp", "dp")
    )
    placed = (
        P("dp", SP_TP, None),
        P("dp", None),
        P("dp", SP, None),
        P(),
        P(None, SP, "tp"),
        P(),
        P("dp", "tp"),
        P("dp", "tp"),
        P("dp", "tp"),
        P("dp", "tp"),
        P(None, "dp", "tp"),
        P(None, "tp"),
        P(None, "tp"),
        P(None, "tp"),
        P(None, "tp"),
        P("tp"),
        P(("tp", "dp"), None),
    )
    return jax.shard_map(
        shards, mesh=torus, in_specs=placed, out_specs=P("dp", SP_TP, None), check_vma=False
    )
```

profile of v0, /device:TPU:1, one launch (start us, length us, event | category | flops | bytes accessed | tf_op | source)
XLA Modules:
  0.0 347.1 jit_solution(8498954441574411239)
XLA Ops:
  7.7 5.4 %concatenate.20 = bf16[1024,1296]{1,0:T(8,128)(2,1)} concatenate(bf16[1024,512]{1,0:T(8,128)(2,1)} %param.23, bf16[1024,128]{1,0:T(8,128)(2,1)} %param.24, bf16[1024,128]{1,0:T(8,128)(2,1)} %param.25, bf16[1024,512]{1,0:T(8,128)(2,1)} %param.26, bf16[1024,8]{1,0:T(8,128)(2,1)S(1)} %copy.97, bf16[1024,8]{1,0:T(8,128)(2,1)S(1)} %copy.98), dimensions={1} | concatenate | bytes 5308416 | tf_op jit(solution)/shard_map/concatenate | solution.py:42
  14.0 29.8 %psum.14 = f32[3,2,512]{2,1,0:T(2,128)S(1)} all-reduce(f32[3,2,512]{2,1,0:T(2,128)S(1)} %convolution_bitcast_fusion.4), channel_id=1, replica_groups=mesh['sp_0'=8,'sp_1'=8,'tp'=4,'dp'=2] {'sp_0'}, use_global_device_ids=true, to_apply=%region_0.1 | all-reduce | flops 3072 | bytes 24576 | tf_op jit(solution)/shard_map/psum | solution.py:19
  43.8 23.1 %psum.15 = f32[3,2,512]{2,1,0:T(2,128)S(1)} all-reduce(f32[3,2,512]{2,1,0:T(2,128)S(1)} %psum.14), channel_id=1, replica_groups=mesh['sp_0'=8,'sp_1'=8,'tp'=4,'dp'=2] {'sp_1'}, use_global_device_ids=true, to_apply=%region_1.2 | all-reduce | flops 3072 | bytes 24576 | tf_op jit(solution)/shard_map/psum | solution.py:19
  67.5 4.0 %all-to-all-start = ((f32[4,3,2,512]{3,2,1,0:T(2,128)}), f32[4,3,2,512]{3,2,1,0:T(2,128)S(1)}, u32[]{:S(2)}, u32[]{:S(2)}) async-start(f32[4,3,2,512]{3,2,1,0:T(2,128)} %broadcast_in_dim.22), calls=%async_computation | async-start | bytes 98304 | tf_op jit(solution)/shard_map/all_to_all | solution.py:30
  71.7 4.2 %all-to-all-done = f32[4,3,2,512]{3,2,1,0:T(2,128)S(1)} async-done(((f32[4,3,2,512]{3,2,1,0:T(2,128)}), f32[4,3,2,512]{3,2,1,0:T(2,128)S(1)}, u32[]{:S(2)}, u32[]{:S(2)}) %all-to-all-start) | async-done | bytes 49184 | tf_op jit(solution)/shard_map/all_to_all | solution.py:30
  77.5 4.1 %all-to-all-start.1 = ((bf16[4,32,2048]{2,1,0:T(8,128)(2,1)}), bf16[4,32,2048]{2,1,0:T(8,128)(2,1)}, u32[]{:S(2)}, u32[]{:S(2)}) async-start(bf16[4,32,2048]{2,1,0:T(8,128)(2,1)} %broadcast_in_dim.24), calls=%async_computation.1 | async-start | bytes 1048576 | tf_op jit(solution)/shard_map/all_to_all | solution.py:30
  83.8 3.1 split.20
  88.9 9.4 %concatenate.21 = bf16[2048,1296]{1,0:T(8,128)(2,1)} concatenate(bf16[2048,768]{1,0:T(8,128)(2,1)S(1)} %split.18, bf16[2048,16]{1,0:T(8,128)(2,1)} %split.19, bf16[2048,512]{1,0:T(8,128)(2,1)} %split.20), dimensions={1} | concatenate | bytes 10616832 | tf_op jit(solution)/shard_map/concatenate | solution.py:237
  98.3 5.1 %convolution_convert_fusion.1 = bf16[128,1296]{0,1:T(8,128)(2,1)S(1)} fusion(bf16[128,2048]{1,0:T(8,128)(2,1)} %bitcast.7, bf16[2048,1296]{1,0:T(8,128)(2,1)} %concatenate.21), kind=kOutput, calls=%fused_computation.5 | convolution fusion | flops 679643136 | bytes 6164480 | tf_op jit(solution)/shard_map/dot_general | solution.py:261
  109.1 3.8 %collective-permute-done.1 = bf16[1,768]{0,1:T(8,128)(2,1)S(1)} collective-permute-done((bf16[1,768]{0,1:T(8,128)(2,1)S(1)}, bf16[1,768]{0,1:T(8,128)(2,1)S(1)}, u32[]{:S(2)}, u32[]{:S(2)}) %collective-permute-start.1) | collective-permute-done | bytes 1568 | tf_op jit(solution)/shard_map/ppermute | solution.py:54
  118.5 13.1 %all_gather.48 = bf16[8,1,8]{2,1,0:T(2,128)(2,1)S(1)} all-gather(bf16[1,1,8]{2,1,0:T(2,128)(2,1)S(1)} %slice.999), channel_id=1, replica_groups=mesh['sp_0'=8,'sp_1'=8,'tp'=4,'dp'=2] {'sp_1'}, dimensions={0}, use_global_device_ids=true | all-gather | bytes 144 | tf_op jit(solution)/shard_map/all_gather | solution.py:71
  131.7 35.6 %all-gather.19.cloned.1.call-done = bf16[64,64,128]{2,1,0:T(8,128)(2,1)} async-done(((bf16[8,64,128]{2,1,0:T(8,128)(2,1)}), bf16[64,64,128]{2,1,0:T(8,128)(2,1)}) %all-gather.19.cloned.1.call-update) | async-done | bytes 1048592 | tf_op jit(solution)/shard_map/all_gather | solution.py:71
  169.6 11.2 %all_gather.43 = bf16[8,1,8]{2,1,0:T(2,128)(2,1)S(1)} all-gather(bf16[1,1,8]{2,1,0:T(2,128)(2,1)S(1)} %slice.1000), channel_id=1, replica_groups=mesh['sp_0'=8,'sp_1'=8,'tp'=4,'dp'=2] {'sp_1'}, dimensions={0}, use_global_device_ids=true | all-gather | bytes 144 | tf_op jit(solution)/shard_map/all_gather | solution.py:71
  180.9 28.2 %all-gather.17.cloned.1.call-done = bf16[64,64,128]{2,1,0:T(8,128)(2,1)} async-done(((bf16[8,64,128]{2,1,0:T(8,128)(2,1)}), bf16[64,64,128]{2,1,0:T(8,128)(2,1)}) %all-gather.17.cloned.1.call-update) | async-done | bytes 1048592 | tf_op jit(solution)/shard_map/all_gather | solution.py:71
  213.4 13.5 %all_gather.49 = bf16[8,1,8]{2,1,0:T(2,128)(2,1)S(1)} all-gather(bf16[1,1,8]{2,1,0:T(2,128)(2,1)S(1)} %get-tuple-element.103), channel_id=1, replica_groups=mesh['sp_0'=8,'sp_1'=8,'tp'=4,'dp'=2] {'sp_0'}, dimensions={0}, use_global_device_ids=true | all-gather | bytes 144 | tf_op jit(solution)/shard_map/all_gather | solution.py:71
  227.6 10.5 %all_gather.44 = bf16[8,1,8]{2,1,0:T(2,128)(2,1)S(1)} all-gather(bf16[1,1,8]{2,1,0:T(2,128)(2,1)S(1)} %get-tuple-element.83), channel_id=1, replica_groups=mesh['sp_0'=8,'sp_1'=8,'tp'=4,'dp'=2] {'sp_0'}, dimensions={0}, use_global_device_ids=true | all-gather | bytes 144 | tf_op jit(solution)/shard_map/all_gather | solution.py:71
  242.2 8.2 %all-to-all-start.2 = ((bf16[64,8,656]{2,1,0:T(8,128)(2,1)}), bf16[64,8,656]{2,1,0:T(8,128)(2,1)S(1)}, u32[]{:S(2)}, u32[]{:S(2)}) async-start(bf16[64,8,656]{2,1,0:T(8,128)(2,1)} %broadcast_in_dim.26), calls=%async_computation.2 | async-start | bytes 1572864 | tf_op jit(solution)/shard_map/all_to_all | solution.py:30
  255.4 11.4 %all-to-all-done.2 = bf16[64,8,656]{2,1,0:T(8,128)(2,1)S(1)} async-done(((bf16[64,8,656]{2,1,0:T(8,128)(2,1)}), bf16[64,8,656]{2,1,0:T(8,128)(2,1)S(1)}, u32[]{:S(2)}, u32[]{:S(2)}) %all-to-all-start.2) | async-done | bytes 671776 | tf_op jit(solution)/shard_map/all_to_all | solution.py:30
  277.3 6.3 %rev.35 = bf16[512,512]{1,0:T(8,128)(2,1)S(1)} reverse(bf16[512,512]{1,0:T(8,128)(2,1)} %get-tuple-element.48), dimensions={0} | reverse | bytes 1048576 | tf_op jit(solution)/shard_map/jit(_flip)/rev | solution.py:254
  284.7 3.3 fusion.13
  289.7 10.8 %all-gather.11.cloned.1.call-done = bf16[8,1,8,64,128]{4,3,2,1,0:T(8,128)(2,1)} async-done(((bf16[1,1,8,64,128]{4,3,2,1,0:T(8,128)(2,1)}), bf16[8,1,8,64,128]{4,3,2,1,0:T(8,128)(2,1)}) %all-gather.11.cloned.1.call-update) | async-done | bytes 1048592 | tf_op jit(solution)/shard_map/all_gather | solution.py:71
  300.8 2.6 fusion.12
  303.9 21.7 %all-gather.15.cloned.1.call-done = bf16[512,2048]{1,0:T(8,128)(2,1)} async-done(((bf16[256,2048]{1,0:T(8,128)(2,1)}), bf16[512,2048]{1,0:T(8,128)(2,1)}) %all-gather.15.cloned.1.call-update) | async-done | bytes 2097168 | tf_op jit(solution)/shard_map/all_gather | solution.py:227
  327.7 11.9 %all_to_all.20 = bf16[4,32,2048]{2,1,0:T(8,128)(2,1)S(1)} all-to-all(bf16[4,32,2048]{2,1,0:T(8,128)(2,1)S(1)} %bitcast.494), channel_id=1, replica_groups=mesh['sp_0'=8,'sp_1'=8,'tp'=4,'dp'=2] {'tp'}, dimensions={0} | all-to-all | bytes 1048576 | tf_op jit(solution)/shard_map/all_to_all | solution.py:93
  (295 shorter events, 52.0 us)
Async XLA Ops:
  6.5 75.3 %all-gather.9.cloned.1.call-start = ((), (), s32[]{:S(2)}) async-start(), calls=%async_computation.4 | async-start | bytes 8650752 | tf_op jit(solution)/shard_map/all_gather | solution.py:43
  13.1 58.5 %copy-start.3 = (bf16[1,32,2048]{2,1,0:T(8,128)(2,1)S(1)}, bf16[1,32,2048]{2,1,0:T(8,128)(2,1)}, u32[]{:S(2)}) copy-start(bf16[1,32,2048]{2,1,0:T(8,128)(2,1)} %param.17) | copy-start | bytes 393220
  13.1 58.6 %copy-start.25 = (bf16[2048]{0:T(1024)(128)(2,1)S(1)}, bf16[2048]{0:T(1024)(128)(2,1)}, u32[]{:S(2)}) copy-start(bf16[2048]{0:T(1024)(128)(2,1)} %param.22) | copy-start | bytes 12292
  13.1 68.6 %copy-start.15 = (bf16[3,512]{1,0:T(4,128)(2,1)S(1)}, bf16[3,512]{1,0:T(4,128)(2,1)}, u32[]{:S(2)}) copy-start(bf16[3,512]{1,0:T(4,128)(2,1)} %param.28) | copy-start | bytes 9220
  13.1 68.6 %copy-start.30 = (bf16[3,128]{1,0:T(4,128)(2,1)S(1)}, bf16[3,128]{1,0:T(4,128)(2,1)}, u32[]{:S(2)}) copy-start(bf16[3,128]{1,0:T(4,128)(2,1)} %param.29) | copy-start | bytes 2308
  13.1 68.6 %copy-start.66 = (bf16[3,128]{1,0:T(4,128)(2,1)S(1)}, bf16[3,128]{1,0:T(4,128)(2,1)}, u32[]{:S(2)}) copy-start(bf16[3,128]{1,0:T(4,128)(2,1)} %param.30) | copy-start | bytes 2308
  13.1 68.7 %copy-start.68 = (f32[2,8]{1,0:T(2,128)S(1)}, f32[2,8]{1,0:T(2,128)}, u32[]{:S(2)}) copy-start(f32[2,8]{1,0:T(2,128)} %param.31) | copy-start | bytes 196
  67.5 8.4 %all-to-all-start = ((f32[4,3,2,512]{3,2,1,0:T(2,128)}), f32[4,3,2,512]{3,2,1,0:T(2,128)S(1)}, u32[]{:S(2)}, u32[]{:S(2)}) async-start(f32[4,3,2,512]{3,2,1,0:T(2,128)} %broadcast_in_dim.22), calls=%async_computation | async-start | bytes 98304 | tf_op jit(solution)/shard_map/all_to_all | solution.py:30
  77.5 20.8 %all-to-all-start.1 = ((bf16[4,32,2048]{2,1,0:T(8,128)(2,1)}), bf16[4,32,2048]{2,1,0:T(8,128)(2,1)}, u32[]{:S(2)}, u32[]{:S(2)}) async-start(bf16[4,32,2048]{2,1,0:T(8,128)(2,1)} %broadcast_in_dim.24), calls=%async_computation.1 | async-start | bytes 1048576 | tf_op jit(solution)/shard_map/all_to_all | solution.py:30
  81.7 85.5 %all-gather.19.cloned.1.call-start = ((), (), s32[]{:S(2)}) async-start(), calls=%async_computation.9 | async-start | bytes 1179648 | tf_op jit(solution)/shard_map/all_gather | solution.py:71
  104.8 4.3 %collective-permute-start = (bf16[1,768]{0,1:T(8,128)(2,1)S(1)}, bf16[1,768]{0,1:T(8,128)(2,1)S(1)}, u32[]{:S(2)}, u32[]{:S(2)}) collective-permute-start(bf16[1,768]{0,1:T(8,128)(2,1)S(1)} %get-tuple-element.49), channel_id=1, source_target_pairs={{0,8},{8,16},{16,24},{24,32},{32,40},{40,48},{48,56},{56,64},{64,7... | collective-permute-start | bytes 4616 | tf_op jit(solution)/shard_map/ppermute | solution.py:53
  106.5 6.4 %collective-permute-start.1 = (bf16[1,768]{0,1:T(8,128)(2,1)S(1)}, bf16[1,768]{0,1:T(8,128)(2,1)S(1)}, u32[]{:S(2)}, u32[]{:S(2)}) collective-permute-start(bf16[1,768]{0,1:T(8,128)(2,1)S(1)} %get-tuple-element.50), channel_id=1, source_target_pairs={{8,0},{16,8},{24,16},{32,24},{40,32},{48,40},{56,48},{64,56},{72,6... | collective-permute-start | bytes 4616 | tf_op jit(solution)/shard_map/ppermute | solution.py:54
  115.9 93.1 %all-gather.17.cloned.1.call-start = ((), (), s32[]{:S(2)}) async-start(), calls=%async_computation.8 | async-start | bytes 1179648 | tf_op jit(solution)/shard_map/all_gather | solution.py:71
  117.5 94.5 %copy-start.16 = (bf16[3,512]{1,0:T(4,128)(2,1)S(1)}, bf16[3,512]{1,0:T(4,128)(2,1)}, u32[]{:S(2)}) copy-start(bf16[3,512]{1,0:T(4,128)(2,1)} %param.28) | copy-start | bytes 9220
  117.6 94.5 %copy-start.31 = (bf16[3,128]{1,0:T(4,128)(2,1)S(1)}, bf16[3,128]{1,0:T(4,128)(2,1)}, u32[]{:S(2)}) copy-start(bf16[3,128]{1,0:T(4,128)(2,1)} %param.29) | copy-start | bytes 2308
  117.6 95.1 %copy-start.11 = (bf16[1,8,2048]{2,1,0:T(8,128)(2,1)S(1)}, bf16[1,8,2048]{2,1,0:T(8,128)(2,1)}, u32[]{:S(2)}) copy-start(bf16[1,8,2048]{2,1,0:T(8,128)(2,1)} %param.19) | copy-start | bytes 98308
  117.6 95.2 %copy-start.67 = (bf16[512]{0:T(512)(128)(2,1)S(1)}, bf16[512]{0:T(512)(128)(2,1)}, u32[]{:S(2)}) copy-start(bf16[512]{0:T(512)(128)(2,1)} %param.32) | copy-start | bytes 3076
  118.5 165.9 %all-gather.13.cloned.1.call-start = ((), (), s32[]{:S(2)}) async-start(), calls=%async_computation.6 | async-start | bytes 1179648 | tf_op jit(solution)/shard_map/all_gather | solution.py:71
  169.5 131.0 %all-gather.11.cloned.1.call-start = ((), (), s32[]{:S(2)}) async-start(), calls=%async_computation.5 | async-start | bytes 1179648 | tf_op jit(solution)/shard_map/all_gather | solution.py:71
  180.8 57.9 %copy-start.37 = (f32[8]{0:T(128)}, f32[8]{0:T(128)S(1)}, u32[]{:S(2)}) copy-start(f32[8]{0:T(128)S(1)} %get-tuple-element.86) | copy-start | bytes 100
  180.8 57.9 %copy-start.39 = (f32[8]{0:T(128)}, f32[8]{0:T(128)S(1)}, u32[]{:S(2)}) copy-start(f32[8]{0:T(128)S(1)} %get-tuple-element.87) | copy-start | bytes 100
  180.9 57.9 %copy-start.41 = (f32[8]{0:T(128)}, f32[8]{0:T(128)S(1)}, u32[]{:S(2)}) copy-start(f32[8]{0:T(128)S(1)} %get-tuple-element.88) | copy-start | bytes 100
  211.4 114.2 %all-gather.15.cloned.1.call-start = ((), (), s32[]{:S(2)}) async-start(), calls=%async_computation.7 | async-start | bytes 3145728 | tf_op jit(solution)/shard_map/all_gather | solution.py:227
  242.2 24.7 %all-to-all-start.2 = ((bf16[64,8,656]{2,1,0:T(8,128)(2,1)}), bf16[64,8,656]{2,1,0:T(8,128)(2,1)S(1)}, u32[]{:S(2)}, u32[]{:S(2)}) async-start(bf16[64,8,656]{2,1,0:T(8,128)(2,1)} %broadcast_in_dim.26), calls=%async_computation.2 | async-start | bytes 1572864 | tf_op jit(solution)/shard_map/all_to_all | solution.py:30
  (71 other events, 1120.1 us)
Sparse Core Ops, SparseCore 0:
  13.3 31.0 all-gather.8
  116.1 51.1 all-gather.18
  169.3 39.7 all-gather.16
  211.0 41.0 all-gather.12
  254.0 46.4 all-gather.10
  302.5 22.9 all-gather.14
where the time goes:
time: 349 us; the launch traced here: 347 us
  waiting for transfers between devices  117 us (34%)
  blocking collectives  113 us (32%)
  local copies, waits for them, and re-layouts  40.7 us (12%)
  other arithmetic  23 us (7%)
  starting transfers between devices  19.6 us (6%)
  matrix products  18.9 us (5%)
  between operations  15 us (4%)
    all_gather x4, waiting for transfers between devices, entering_2(): lax.all_gather(part.astype(kind), axis)  74.5 us
    psum x2, blocking collectives, over_axes(): return functools.reduce(lax.psum, axes, x)  52.9 us
    all_gather x4, blocking collectives, entering_2(): lax.all_gather(part.astype(kind), axis)  48.2 us
    all_gather x1, waiting for transfers between devices, shards(): lax.all_gather(w_out, 'dp', axis=0, tiled=True)  21.7 us
    all_to_all x3, starting transfers between devices, sent_to_all(): lax.all_to_all(jnp.broadcast_to(x[None], (peers, *x.shape)), axis, 0, 0,...  16.4 us
    all_to_all x3, waiting for transfers between devices, sent_to_all(): lax.all_to_all(jnp.broadcast_to(x[None], (peers, *x.shape)), axis, 0, 0,...  15.7 us
    all_to_all x1, blocking collectives, sum_at_owner(): tiles = lax.all_to_all(split_up(x, dim, peers), axis, 0, 0, tiled=True)  11.9 us
    concatenate x1, local copies, waits for them, and re-layouts, shards(): jnp.concatenate([full_x, full_b, full_c, full_fwd, full_bwd, full_z], axi...  9.42 us
  transfers between devices with their start and end apart: 11, of which 8 were waited for; matrix products, arithmetic and copies ran while one was open for 18% of the time, Pallas kernels for 0%

commit v1 on v0

v1 whole, which is shorter than its diff:
```python
import functools

import jax
import jax.numpy as jnp
from jax import lax
from jax.experimental import pallas as pl
from jax.experimental.pallas import tpu as pltpu
from jax.sharding import Mesh
from jax.sharding import PartitionSpec as P

F32 = jnp.float32
BF16 = jnp.bfloat16
MESH = pl.DeviceIdType.MESH
EPS = 1e-06
NZ = 8
NY = 8
NSP = 64
TP = 4
ROWS = 32
TOK = 128
CTXR = 8
D = 2048
M = 144


def dot(a, b):
    return jnp.dot(a, b, preferred_element_type=F32)


def tdot(a, b):
    return lax.dot_general(a, b, (((0,), (0,)), ((), ())), preferred_element_type=F32)


def iota(shape, dim):
    return lax.broadcasted_iota(jnp.int32, shape, dim)


def silu(v):
    return v / (1.0 + jnp.exp(-v))


def softplus(v):
    return jnp.maximum(v, 0.0) + jnp.log1p(jnp.exp(-jnp.abs(v)))


def high_low(v, shift):
    high = v.astype(BF16).astype(F32)
    low = (v - high).astype(BF16).astype(F32)
    return (high + pltpu.roll(low, shift, 1)).astype(BF16)


def kernel(
    latent,
    condition,
    context,
    source,
    mod_w,
    gain,
    w_x,
    w_b,
    w_c,
    w_z,
    w_dt,
    taps_x,
    taps_b,
    taps_c,
    rates,
    out_gain,
    w_out,
    out,
    v_lat,
    v_cond,
    v_ctx,
    v_src,
    v_mod,
    v_gain,
    v_w,
    v_dt,
    v_tx,
    v_tb,
    v_tc,
    v_rate,
    v_og,
    v_wo,
    v_p,
    v_my,
    v_mz,
    v_ms,
    v_mx,
    v_edge,
    v_halo,
    v_h,
    v_f,
    v_pdt,
    v_e,
    v_cts,
    v_ctr,
    v_s,
    v_r,
    v_dec,
    v_t,
    v_o,
    v_hin,
    v_y,
    v_ny,
    v_po,
    v_pr,
    loc_sem,
    ws_sem,
    wr_sem,
    ls_sem,
    lr_sem,
    ys_sem,
    yr_sem,
    zs_sem,
    zr_sem,
    xs_sem,
    xr_sem,
    hs_sem,
    hr_sem,
    a_sem,
    p_ssem,
    p_rsem,
):
    z = lax.axis_index("sp_0")
    y = lax.axis_index("sp_1")
    t = lax.axis_index("tp")
    c = lax.axis_index("dp")
    k = z * NY + y

    barrier = pltpu.get_barrier_semaphore()
    after = lax.rem(k + 1, NSP)
    before = lax.rem(k + NSP - 1, NSP)
    after_id = {"sp_0": after // NY, "sp_1": lax.rem(after, NY)}
    before_id = {"sp_0": before // NY, "sp_1": lax.rem(before, NY)}
    for d in (4, 3, 5, 2, 6, 1, 7):
        pl.semaphore_signal(barrier, 1, device_id={"sp_1": lax.rem(y + d, NY)}, device_id_type=MESH)
        pl.semaphore_signal(barrier, 1, device_id={"sp_0": lax.rem(z + d, NZ)}, device_id_type=MESH)
    for d in (2, 1, 3):
        pl.semaphore_signal(barrier, 1, device_id={"tp": lax.rem(t + d, TP)}, device_id_type=MESH)
    pl.semaphore_signal(barrier, 1, device_id={"dp": 1 - c}, device_id_type=MESH)
    pl.semaphore_signal(barrier, 1, device_id=after_id, device_id_type=MESH)
    pl.semaphore_signal(barrier, 1, device_id=before_id, device_id_type=MESH)

    half = pl.ds(pl.multiple_of(c * 1024, 1024), 1024)
    whalf = pl.ds(pl.multiple_of(c * 256, 256), 256)
    small = [
        (condition, v_cond),
        (source, v_src),
        (mod_w, v_mod),
        (latent.at[0], v_lat.at[t]),
        (context.at[0], v_ctx),
        (gain, v_gain),
        (taps_x, v_tx),
        (taps_b, v_tb),
        (taps_c, v_tc),
        (rates, v_rate),
        (out_gain, v_og),
    ]
    weights = [
        (w_dt, v_dt.at[:, half, :]),
        (w_b, v_w.at[2, half, 0:128]),
        (w_c, v_w.at[2, half, 128:256]),
        (w_x.at[:, 0:256], v_w.at[0, half, :]),
        (w_x.at[:, 256:512], v_w.at[1, half, :]),
        (w_z.at[:, 0:256], v_w.at[3, half, :]),
        (w_z.at[:, 256:512], v_w.at[4, half, :]),
        (w_out, v_wo.at[whalf, :]),
    ]
    local = [
        pltpu.make_async_copy(a, b, loc_sem.at[i]) for i, (a, b) in enumerate(small + weights)
    ]
    for copy in local:
        copy.start()

    pl.semaphore_wait(barrier, 20)

    def remote(a, b, ssem, rsem, where):
        return pltpu.make_async_remote_copy(
            src_ref=a, dst_ref=b, send_sem=ssem, recv_sem=rsem, device_id=where, device_id_type=MESH
        )

    local[0].wait()
    local[1].wait()
    local[2].wait()
    lane0 = pl.ds(pl.multiple_of((k // 4) * 128, 128), 128)
    shift = lax.rem(128 - lax.rem(k, 4) * 32, 128)

    def own_act(ref):
        act = silu(ref[0:1, lane0].astype(F32)).astype(BF16).astype(F32)
        return pltpu.roll(jnp.broadcast_to(act, (8, 128)), shift, 1)

    act_lat = own_act(v_cond)
    act_ctx = own_act(v_src)
    row8 = iota((8, 128), 0)
    zero8 = jnp.zeros((8, 128), F32)
    lhs = (
        jnp.where(row8 == 0, act_lat, jnp.where(row8 == 3, act_ctx, zero8)),
        jnp.where(row8 == 1, act_lat, jnp.where(row8 == 4, act_ctx, zero8)),
        jnp.where(row8 == 2, act_lat, zero8),
    )
    partial = sum(dot(lhs[i][:, 0:32].astype(BF16), v_mod[i]) for i in range(3))
    v_p[...] = partial

    def exchange(src, slots, axis, me, peers, ssem, rsem):
        order = sorted(range(1, peers), key=lambda d: -min(d, peers - d))
        copies = [
            remote(src, slots.at[d], ssem.at[d], rsem.at[d], {axis: lax.rem(me + d, peers)})
            for d in order
        ]
        for copy in copies:
            copy.start()
        return copies

    y_copies = exchange(v_p, v_my, "sp_1", y, NY, ys_sem, yr_sem)

    lat_copies = [
        remote(
            latent.at[0], v_lat.at[t], ls_sem.at[d], lr_sem.at[d], {"tp": lax.rem(t + d, TP)}
        )
        for d in (2, 1, 3)
    ]
    for copy in lat_copies:
        copy.start()
    w_copies = [
        remote(a, b, ws_sem.at[i], wr_sem.at[i], {"dp": 1 - c}) for i, (a, b) in enumerate(weights)
    ]
    for copy in w_copies:
        copy.start()

    r_e = iota((32, 1024), 0)
    l_e = iota((32, 1024), 1)
    hit = lax.bitwise_and(r_e, 15) == (
        lax.bitwise_and(lax.shift_right_logical(l_e, 6), 1) * 8 + lax.shift_right_logical(l_e, 7)
    )
    v_e[...] = jnp.where(hit, 1.0, 0.0).astype(BF16)
    v_pdt[...] = jnp.zeros((M, 128), F32)

    for copy in y_copies:
        copy.wait_recv()
    v_ms[0] = v_p[...] + sum(v_my[d] for d in range(1, NY))
    z_copies = exchange(v_ms.at[0], v_mz, "sp_0", z, NZ, zs_sem, zr_sem)

    local[3].wait()
    for copy in lat_copies:
        copy.wait_recv()
    v_edge[0] = v_lat[0, 0:8, :].astype(F32)[0:1]
    v_edge[1] = v_lat[TP - 1, 24:32, :].astype(F32)[7:8]
    last_copy = remote(v_edge.at[1], v_halo.at[0], hs_sem.at[0], hr_sem.at[0], after_id)
    first_copy = remote(v_edge.at[0], v_halo.at[1], hs_sem.at[1], hr_sem.at[1], before_id)
    last_copy.start()
    first_copy.start()

    def inverse(rows):
        return lax.rsqrt(jnp.mean(rows * rows, axis=-1, keepdims=True) + EPS)

    inv_lat = [inverse(v_lat[i].astype(F32)) for i in range(TP)]

    for copy in z_copies:
        copy.wait_recv()
    v_ms[1] = v_ms[0] + sum(v_mz[d] for d in range(1, NZ))
    v_mx[t] = v_ms[1]
    x_copies = [
        remote(v_ms.at[1], v_mx.at[t], xs_sem.at[d], xr_sem.at[d], {"tp": lax.rem(t + d, TP)})
        for d in (2, 1, 3)
    ]
    for copy in x_copies:
        copy.start()
    for i in range(4, len(local)):
        local[i].wait()
    ctx_rows = v_ctx[...].astype(F32)
    inv_ctx = inverse(ctx_rows)
    last_copy.wait_recv()
    first_copy.wait_recv()
    row_h = iota((8, D), 0)
    halo = jnp.where(row_h == 0, v_halo[0], jnp.where(row_h == 1, v_halo[1], jnp.zeros((8, D), F32)))
    inv_halo = inverse(halo)
    for copy in w_copies:
        copy.wait_recv()
    for copy in x_copies:
        copy.wait_recv()

    for j in range(TP):
        cols = slice(j * 512, (j + 1) * 512)
        mods = v_mx[j]
        gain_j = v_gain[0:1, cols].astype(F32)
        mul = gain_j * (1.0 + mods[1:2])
        add = mods[0:1]
        for i in range(TP):
            rows = v_lat[i, :, cols].astype(F32)
            v_h[i * ROWS : (i + 1) * ROWS, cols] = (rows * inv_lat[i] * mul + add).astype(BF16)
        ctx_h = ctx_rows[:, cols] * inv_ctx * (gain_j * (1.0 + mods[4:5])) + mods[3:4]
        halo_h = halo[:, cols] * inv_halo * mul + add
        v_h[TOK:M, cols] = jnp.concatenate([ctx_h, halo_h], axis=0).astype(BF16)

    v_pdt[:, 0:8] = dot(v_h[...], v_dt[0])
    v_pdt[:, 8:16] = dot(v_h[...], v_dt[1])
    for i in (2, 0, 1):
        v_f[i] = dot(v_h[...], v_w[i])

    lane = iota((TOK, 128), 1)
    row = iota((TOK, 128), 0)
    lane8 = iota((8, 128), 1)
    lane16 = iota((16, 128), 1)
    rate = v_rate[...]
    step = softplus(v_pdt[0:TOK])
    decay = -rate * step
    parts = high_low(decay, 16)
    lower = jnp.where(row >= lane, 1.0, 0.0).astype(BF16)
    upper = jnp.where(row <= lane, 1.0, 0.0).astype(BF16)
    cum = jnp.where(lax.bitwise_and(lane, 15) < 8, dot(lower, parts), dot(upper, parts))
    cum = jnp.where(lane < 16, cum + pltpu.roll(cum, 112, 1), 0.0)
    total = jnp.where(lane8[0:1] < 8, cum[TOK - 1 : TOK], cum[0:1])

    total8 = jnp.broadcast_to(total, (8, 128))
    total_hi = total8.astype(BF16).astype(F32)
    total_lo = total8 - total_hi
    tail = v_pdt[TOK : TOK + 8]
    tail = tail + pltpu.roll(total_hi, 16, 1) + pltpu.roll(total_lo, 32, 1)
    tail = pltpu.roll(tail, 80, 1)
    ctx_b = v_f[2, TOK : TOK + 8, 0:128]
    b_tiles = [pltpu.roll(ctx_b, (64 - 16 * n) % 128, 1) for n in range(8)]
    for h in range(8):
        x_tile = v_f[h // 4, TOK : TOK + 8, ((h // 2) % 2) * 128 : ((h // 2) % 2) * 128 + 128]
        if h % 2:
            x_tile = pltpu.roll(x_tile, 64, 1)
        for n in range(8):
            tile = jnp.where(lane8 < 64, x_tile, jnp.where(lane8 < 80, b_tiles[n], tail))
            v_cts[h * 8 + n] = tile.astype(BF16)

    def place(i):
        a = i // 8
        b = lax.rem(i, 8)

        def offset(v):
            halved = (v + 1) // 2
            return jnp.where(lax.rem(v, 2) == 1, 4 - halved, 4 + halved)

        z_to = lax.rem(z + offset(a), NZ)
        y_to = lax.rem(y + offset(b), NY)
        return z_to, y_to

    def all_to_all(src, dst, base):
        def send(i, carry):
            z_to, y_to = place(i)
            remote(
                src.at[z_to * NY + y_to],
                dst.at[k],
                a_sem.at[base],
                a_sem.at[base + 1],
                {"sp_0": z_to, "sp_1": y_to},
            ).start()
            return carry

        lax.fori_loop(0, NSP - 1, send, 0)
        dst[k] = src[k]
        return remote(
            src.at[pl.ds(0, NSP - 1)],
            dst.at[pl.ds(0, NSP - 1)],
            a_sem.at[base],
            a_sem.at[base + 1],
            after_id,
        )

    ctx_wait = all_to_all(v_cts, v_ctr, 0)

    has_before = jnp.where(k > 0, 1.0, 0.0)
    has_after = jnp.where(k < NSP - 1, 1.0, 0.0)

    def conv(i, lo, taps):
        block = v_f[i, 0:TOK, lo : lo + 128]
        ends = v_f[i, TOK + 8 : M, lo : lo + 128]
        prev = ends[0:1] * has_before
        nxt = ends[1:2] * has_after
        down = jnp.where(row == 0, prev, pltpu.roll(block, 1, 0))
        up = jnp.where(row == TOK - 1, nxt, pltpu.roll(block, TOK - 1, 0))
        w = taps.astype(F32)
        return silu(down * w[0:1] + block * w[1:2] + up * w[2:3])

    b_in = conv(2, 0, v_tb[...]).astype(BF16)
    x_in = [conv(p // 2, (p % 2) * 128, v_tx[:, p * 128 : (p + 1) * 128]) for p in range(4)]
    b_turned = b_in.astype(F32).T.astype(BF16)

    to_end = jnp.where(lane < 16, step * jnp.exp(total - cum), 0.0)
    moved = high_low(to_end, 16)[:, 0:32]
    for p in range(4):
        turned = pltpu.roll(x_in[p], 64, 1)
        for s in range(2):
            h = 2 * p + s
            pair = jnp.where(lane < 64, x_in[p], turned) if s == 0 else jnp.where(lane < 64, turned, x_in[p])
            scaled = (pair * dot(moved, v_e[:, h * 128 : (h + 1) * 128])).astype(BF16)
            state = dot(b_turned, scaled).astype(BF16)
            for n in range(8):
                v_s[h * 8 + n] = state[n * 16 : (n + 1) * 16]
    state_wait = all_to_all(v_s, v_r, 2)

    for i in (3, 4):
        v_f[i] = dot(v_h[...], v_w[i])
    c_in = conv(2, 128, v_tc[...]).astype(BF16)
    scores = dot(c_in, b_turned)
    step_t = step.T
    cum_t = cum.T
    for p in range(4):
        x_pair = x_in[p].astype(BF16)
        sides = []
        for s in range(2):
            h = 2 * p + s
            spread = jnp.where(
                row >= lane,
                cum[:, h : h + 1] - cum_t[h : h + 1],
                cum[:, 8 + h : 9 + h] - cum_t[8 + h : 9 + h],
            )
            f_row = step_t[h : h + 1]
            b_row = step_t[8 + h : 9 + h]
            coef = jnp.where(row > lane, f_row, jnp.where(row < lane, b_row, f_row + b_row))
            weight = scores * jnp.exp(jnp.minimum(spread, 0.0)) * coef
            sides.append(dot(weight.astype(BF16), x_pair))
        v_y[p] = jnp.where(lane < 64, sides[0], sides[1])
    growth = high_low(jnp.where(lane < 16, jnp.exp(cum), 0.0), 16)[:, 0:32]

    ctx_wait.wait_recv()
    feats = v_ctr[...].astype(F32).reshape(NSP * CTXR, 128)
    row_c = iota((NSP * CTXR, 128), 0)
    lane_c = iota((NSP * CTXR, 128), 1)
    x_lanes = pl.ds(pl.multiple_of((z // 2) * 128, 128), 128)
    x_shift = lax.rem(z, 2) * 64
    b_shift = lax.rem(192 - 16 * y, 128)

    def owner_tap(i):
        tx = jnp.broadcast_to(v_tx[i : i + 1, x_lanes].astype(F32), (8, 128))
        tb = jnp.broadcast_to(v_tb[i : i + 1].astype(F32), (8, 128))
        return jnp.where(lane8 < 64, pltpu.roll(tx, x_shift, 1), pltpu.roll(tb, b_shift, 1))[0:1]

    down = jnp.where(row_c == 0, 0.0, pltpu.roll(feats, 1, 0))
    up = jnp.where(row_c == NSP * CTXR - 1, 0.0, pltpu.roll(feats, NSP * CTXR - 1, 0))
    smooth = silu(down * owner_tap(0) + feats * owner_tap(1) + up * owner_tap(2))
    picked = pltpu.roll(feats, lax.rem(128 - z, 128), 1)
    used = (lane_c == 80) | (lane_c == 88)
    step_c = softplus(picked)
    rate_c = pltpu.roll(jnp.broadcast_to(rate, (8, 128)), 80 - z, 1)[0:1]
    decay_c = jnp.where(used, -rate_c * step_c, 0.0)
    parts_c = high_low(decay_c, 1)
    run = jnp.zeros((1, 128), F32)
    pieces = []
    for b in range(4):
        piece = dot(lower, parts_c[b * 128 : (b + 1) * 128]) + run
        run = piece[127:128]
        pieces.append(piece)
    prefix = jnp.concatenate(pieces, axis=0)
    prefix = prefix + pltpu.roll(prefix, 127, 1)
    end = prefix[NSP * CTXR - 1 :]
    reach = jnp.where(lane_c < 84, end - prefix, prefix - decay_c)
    weight_c = jnp.where(used, step_c * jnp.exp(jnp.where(used, reach, 0.0)), 0.0)
    smooth = smooth.astype(BF16)
    x_wide = smooth.astype(F32)
    spread_x = jnp.where(
        lane_c < 64, x_wide * weight_c[:, 80:81], pltpu.roll(x_wide, 64, 1) * weight_c[:, 88:89]
    )
    context_state = tdot(smooth, spread_x.astype(BF16))[64:80]
    grow = jnp.exp(jnp.where((lane_c >= 96) & (lane_c < 112), picked + pltpu.roll(picked, 112, 1), 0.0))
    v_dec[...] = jnp.where(lane_c < 64, grow[:, 96:97], grow[:, 104:105]).reshape(NSP, 8, 128)

    state_wait.wait_recv()

    def advance(i, carry):
        j = NSP - 1 - i
        v_t[i] = carry
        new = jnp.where(lane16 < 64, v_r[i].astype(F32), v_r[j].astype(F32))
        scale = jnp.where(lane8 < 64, v_dec[i], v_dec[j])
        return carry * jnp.concatenate([scale, scale], axis=0) + new

    lax.fori_loop(0, NSP, advance, context_state, unroll=8)

    def collect(i, carry):
        v_o[i] = jnp.where(lane16 < 64, v_t[i], v_t[NSP - 1 - i]).astype(BF16)
        return carry

    lax.fori_loop(0, NSP, collect, 0, unroll=8)
    back_wait = all_to_all(v_o, v_hin, 4)

    back_wait.wait_recv()
    squares = jnp.zeros((TOK, 1), F32)
    gated = []
    for p in range(4):
        sides = []
        for s in range(2):
            h = 2 * p + s
            entering = v_hin[h * 8 : (h + 1) * 8].reshape(128, 128)
            carried = dot(c_in, entering) * dot(growth, v_e[:, h * 128 : (h + 1) * 128])
            sides.append(carried + pltpu.roll(carried, 64, 1))
        gate_in = v_f[3 + p // 2, 0:TOK, (p % 2) * 128 : (p % 2) * 128 + 128]
        value = (v_y[p] + jnp.where(lane < 64, sides[0], sides[1])) * silu(gate_in)
        squares = squares + jnp.sum(value * value, axis=-1, keepdims=True)
        gated.append(value)
    inv = lax.rsqrt(squares / 512.0 + EPS)
    for p in range(4):
        cols = slice(p * 128, (p + 1) * 128)
        v_ny[:, cols] = (gated[p] * inv * v_og[0:1, cols].astype(F32)).astype(BF16)

    out_copies = []
    for n in range(2):
        for q in range(4):
            lo = n * 1024 + q * 256
            term = dot(v_ny[...], v_wo[:, lo : lo + 256]).astype(BF16)
            for i in range(TP):
                v_po[n, i, :, q * 256 : (q + 1) * 256] = term[i * ROWS : (i + 1) * ROWS]
        for d in (2, 1, 3):
            to = lax.rem(t + d, TP)
            copy = remote(
                v_po.at[n, to], v_pr.at[n, d], p_ssem.at[n, d], p_rsem.at[n, d], {"tp": to}
            )
            copy.start()
            out_copies.append(copy)
    for n in range(2):
        for copy in out_copies[n * 3 : n * 3 + 3]:
            copy.wait_recv()
        for q in range(2):
            cols = slice(q * 512, (q + 1) * 512)
            mixed = v_po[n, t, :, cols].astype(F32)
            for d in range(1, TP):
                mixed = mixed + v_pr[n, d, :, cols].astype(F32)
            j = n * 2 + q
            out[0, :, j * 512 : (j + 1) * 512] = (v_mx[j, 2:3] * mixed).astype(BF16)

    for copy in (
        y_copies + z_copies + x_copies + lat_copies + w_copies + [last_copy, first_copy] + out_copies
    ):
        copy.wait_send()
    ctx_wait.wait_send()
    state_wait.wait_send()
    back_wait.wait_send()


def shards(
    latent,
    condition,
    context,
    context_source,
    mod_weight,
    norm_gain,
    w_x,
    w_b,
    w_c,
    w_z,
    w_dt,
    conv_x,
    conv_b,
    conv_c,
    decay_rate,
    out_gain,
    w_out,
):
    rates = jnp.pad(decay_rate.reshape(1, 16), ((0, 0), (0, 112)))
    dma = pltpu.SemaphoreType.DMA
    vmem = pltpu.VMEM
    scratch = [
        vmem((TP, ROWS, D), BF16),
        vmem((1, D), BF16),
        vmem((CTXR, D), BF16),
        vmem((1, D), BF16),
        vmem((3, 32, 512), BF16),
        vmem((1, D), BF16),
        vmem((5, D, 256), BF16),
        vmem((2, D, 8), BF16),
        vmem((3, 512), BF16),
        vmem((3, 128), BF16),
        vmem((3, 128), BF16),
        vmem((1, 128), F32),
        vmem((1, 512), BF16),
        vmem((512, D), BF16),
        vmem((8, 512), F32),
        vmem((NY, 8, 512), F32),
        vmem((NZ, 8, 512), F32),
        vmem((2, 8, 512), F32),
        vmem((TP, 8, 512), F32),
        vmem((2, 1, D), F32),
        vmem((2, 1, D), F32),
        vmem((M, D), BF16),
        vmem((5, M, 256), F32),
        vmem((M, 128), F32),
        vmem((32, 1024), BF16),
        vmem((NSP, CTXR, 128), BF16),
        vmem((NSP, CTXR, 128), BF16),
        vmem((NSP, 16, 128), BF16),
        vmem((NSP, 16, 128), BF16),
        vmem((NSP, 8, 128), F32),
        vmem((NSP, 16, 128), F32),
        vmem((NSP, 16, 128), BF16),
        vmem((NSP, 16, 128), BF16),
        vmem((4, TOK, 128), F32),
        vmem((TOK, 512), BF16),
        vmem((2, TP, ROWS, 1024), BF16),
        vmem((2, TP, ROWS, 1024), BF16),
        dma((19,)),
        dma((8,)),
        dma((8,)),
        dma((TP,)),
        dma((TP,)),
        dma((NY,)),
        dma((NY,)),
        dma((NZ,)),
        dma((NZ,)),
        dma((TP,)),
        dma((TP,)),
        dma((2,)),
        dma((2,)),
        dma((6,)),
        dma((2, TP)),
        dma((2, TP)),
    ]
    call = pl.pallas_call(
        kernel,
        out_shape=jax.ShapeDtypeStruct((1, ROWS, D), BF16),
        in_specs=[pl.BlockSpec(memory_space=pl.ANY)] * 17,
        out_specs=pl.BlockSpec(memory_space=pltpu.VMEM),
        scratch_shapes=scratch,
        compiler_params=pltpu.CompilerParams(
            collective_id=0, has_side_effects=True, vmem_limit_bytes=50 * 1024 * 1024
        ),
        name="mixer",
    )
    return call(
        latent,
        condition,
        context,
        context_source.reshape(1, D),
        mod_weight,
        norm_gain.reshape(1, D),
        w_x,
        w_b,
        w_c,
        w_z,
        w_dt,
        conv_x,
        conv_b,
        conv_c,
        rates,
        out_gain.reshape(1, 512),
        w_out,
    )


def solution(mesh):
    torus = Mesh(
        mesh.devices.reshape(NZ, NY, TP, 2), ("sp_0", "sp_1", "tp", "dp")
    )
    sp = ("sp_0", "sp_1")
    sp_tp = ("sp_0", "sp_1", "tp")
    placed = (
        P("dp", sp_tp, None),
        P("dp", None),
        P("dp", sp, None),
        P(),
        P(None, sp, "tp"),
        P(),
        P("dp", "tp"),
        P("dp", "tp"),
        P("dp", "tp"),
        P("dp", "tp"),
        P(None, "dp", "tp"),
        P(None, "tp"),
        P(None, "tp"),
        P(None, "tp"),
        P(None, "tp"),
        P("tp"),
        P(("tp", "dp"), None),
    )
    return jax.shard_map(
        shards, mesh=torus, in_specs=placed, out_specs=P("dp", sp_tp, None), check_vma=False
    )
```

time: 349 us -> 66.2 us (0.19)
  waiting for transfers between devices: 117 us -> 0 us
  blocking collectives: 113 us -> 0 us
  Pallas kernels: 0 us -> 57.6 us
  local copies, waits for them, and re-layouts: 40.7 us -> 8.15 us
  other arithmetic: 23 us -> 0 us
  starting transfers between devices: 19.6 us -> 0 us
  matrix products: 18.9 us -> 0 us
  between operations: 15 us -> 0.14 us
    all_gather x6 -> x0, waiting for transfers between devices: 96.2 us -> none  [the longest x4 74.5 us: entering_2(): lax.all_gather(part.astype(kind), axis)]
    pallas_call x0 -> x1, Pallas kernels: none -> 57.6 us  [shards(): call(latent, condition, context, context_source.reshape(1, D), mod_weight...]
    psum x2 -> x0, blocking collectives: 52.9 us -> none  [over_axes(): return functools.reduce(lax.psum, axes, x)]
    all_gather x4 -> x0, blocking collectives: 48.2 us -> none  [entering_2(): lax.all_gather(part.astype(kind), axis)]
    dot_general x12 -> x0, matrix products: 18.9 us -> none  [the longest x2 5.89 us: direction_output(): jnp.einsum('clgn,cghpn->clghp', c_blocks, entering.astype(jnp.bfloat16),...]
    all_to_all x3 -> x0, starting transfers between devices: 16.4 us -> none  [sent_to_all(): lax.all_to_all(jnp.broadcast_to(x[None], (peers, *x.shape)), axis, 0, 0,...]
    all_to_all x3 -> x0, waiting for transfers between devices: 15.7 us -> none  [sent_to_all(): lax.all_to_all(jnp.broadcast_to(x[None], (peers, *x.shape)), axis, 0, 0,...]
    concatenate x2 -> x0, local copies, waits for them, and re-layouts: 14.8 us -> none  [the longest x1 9.42 us: shards(): jnp.concatenate([full_x, full_b, full_c, full_fwd, full_bwd, full_z], axi...]
  transfers between devices with their start and end apart: 11 -> 0, of which waited for: 8 -> 0; matrix products, arithmetic and copies ran while one was open for 18% -> 0% of each run, Pallas kernels for 0% -> 0%
where the time goes in v1:
time: 66.2 us; the launch traced here: 65.9 us
  Pallas kernels  57.6 us (87%)
  local copies, waits for them, and re-layouts  8.15 us (12%)
    pallas_call x1, Pallas kernels, shards(): call(latent, condition, context, context_source.reshape(1, D), mod_weight...  57.6 us
    unnamed x28, local copies, waits for them, and re-layouts  6.67 us

profile of v1, /device:TPU:1, one launch (start us, length us, event | category | flops | bytes accessed | tf_op | source)
XLA Modules:
  0.0 65.9 jit_solution(1578131396747321802)
XLA Ops:
  0.0 0.0 copy-start.11
  0.0 0.8 %reshape.14 = f32[1,16]{1,0:T(1,128)S(1)} reshape(f32[2,8]{1,0:T(2,128)} %param.31) | data formatting | bytes 128 | tf_op jit(solution)/shard_map/reshape | solution.py:553
  0.8 0.7 %reshape.15.out_gain = bf16[1,512]{1,0:T(2,128)(2,1)S(1)} reshape(bf16[512]{0:T(512)(128)(2,1)} %param.32) | data formatting | bytes 2048 | tf_op jit(solution)/shard_map/reshape | solution.py:638
  1.5 0.0 copy-done.11
  1.5 0.0 copy-start.10
  1.5 0.7 copy-done.12
  2.2 0.0 copy-start.2
  2.2 0.0 copy-start.3
  2.2 0.0 copy-start.6
  2.2 1.1 %copy.18.w_dt = bf16[2,1024,8]{2,1,0:T(8,128)(2,1)S(1)} copy(bf16[2,1024,8]{1,2,0:T(8,128)(2,1)} %param.27) | data formatting | bytes 65536 | tf_op args[10]
  3.3 0.0 copy-done.9
  3.3 0.0 copy-done.10
  3.3 0.0 copy-done.7
  3.3 0.0 copy-done.8
  3.3 0.0 copy-done.2
  3.3 0.0 copy-done.3
  3.4 0.0 copy-done.6
  3.4 0.0 copy-start
  3.4 1.2 %copy-done = bf16[1024,512]{1,0:T(8,128)(2,1)S(1)} copy-done((bf16[1024,512]{1,0:T(8,128)(2,1)S(1)}, bf16[1024,512]{1,0:T(8,128)(2,1)}, u32[]{:S(2)}) %copy-start) | copy-done | bytes 1048600
  4.6 1.2 %copy-done.1 = bf16[1024,512]{1,0:T(8,128)(2,1)S(1)} copy-done((bf16[1024,512]{1,0:T(8,128)(2,1)S(1)}, bf16[1024,512]{1,0:T(8,128)(2,1)}, u32[]{:S(2)}) %copy-start.1) | copy-done | bytes 1048600
  5.8 0.9 %copy-done.4 = bf16[1,32,2048]{2,1,0:T(8,128)(2,1)S(1)} copy-done((bf16[1,32,2048]{2,1,0:T(8,128)(2,1)S(1)}, bf16[1,32,2048]{2,1,0:T(8,128)(2,1)}, u32[]{:S(2)}) %copy-start.4) | copy-done | bytes 131096
  6.7 0.9 %copy-done.5 = bf16[3,32,512]{2,1,0:T(8,128)(2,1)S(1)} copy-done((bf16[3,32,512]{2,1,0:T(8,128)(2,1)S(1)}, bf16[3,32,512]{2,1,0:T(8,128)(2,1)}, u32[]{:S(2)}) %copy-start.5) | copy-done | bytes 98328
  7.6 57.6 %mixer.1 = bf16[1,32,2048]{2,1,0:T(8,128)(2,1)S(1)} custom-call(bf16[1,32,2048]{2,1,0:T(8,128)(2,1)S(1)} %copy-done.4, bf16[1,2048]{1,0:T(2,128)(2,1)S(1)} %copy-done.7, bf16[1,8,2048]{2,1,0:T(8,128)(2,1)S(1)} %copy-done.6, bf16[1,2048]{1,0:T(2,128)(2,1)S(1)} %reshape.12.source, bf16[3,32,512]{2,1,0:T(8,128)(2,1)S(1)} %copy-done.5, ...), custom_call_target="tpu_custom_call" | custom-call | tf_op jit(solution)/shard_map/mixer/pallas_call | solution.py:622
  65.2 0.7 copy.20
  (10 shorter events, 0.0 us)
Async XLA Ops:
  0.0 1.5 %copy-start.11 = (bf16[2048]{0:T(1024)(128)(2,1)S(1)}, bf16[2048]{0:T(1024)(128)(2,1)}, u32[]{:S(2)}) copy-start(bf16[2048]{0:T(1024)(128)(2,1)} %param.20) | copy-start | bytes 12292
  1.5 0.7 %copy-start.12 = (bf16[2048]{0:T(1024)(128)(2,1)S(1)}, bf16[2048]{0:T(1024)(128)(2,1)}, u32[]{:S(2)}) copy-start(bf16[2048]{0:T(1024)(128)(2,1)} %param.22) | copy-start | bytes 12292
  1.5 1.8 %copy-start.9 = (bf16[3,128]{1,0:T(4,128)(2,1)S(1)}, bf16[3,128]{1,0:T(4,128)(2,1)}, u32[]{:S(2)}) copy-start(bf16[3,128]{1,0:T(4,128)(2,1)} %taps_b.1) | copy-start | bytes 2308
  1.5 1.8 %copy-start.10 = (bf16[3,128]{1,0:T(4,128)(2,1)S(1)}, bf16[3,128]{1,0:T(4,128)(2,1)}, u32[]{:S(2)}) copy-start(bf16[3,128]{1,0:T(4,128)(2,1)} %taps_c.1) | copy-start | bytes 2308
  2.2 1.2 %copy-start.7 = (bf16[1,2048]{1,0:T(2,128)(2,1)S(1)}, bf16[1,2048]{1,0:T(2,128)(2,1)}, u32[]{:S(2)}) copy-start(bf16[1,2048]{1,0:T(2,128)(2,1)} %condition.1) | copy-start | bytes 12292
  2.2 1.2 %copy-start.8 = (bf16[3,512]{1,0:T(4,128)(2,1)S(1)}, bf16[3,512]{1,0:T(4,128)(2,1)}, u32[]{:S(2)}) copy-start(bf16[3,512]{1,0:T(4,128)(2,1)} %taps_x.1) | copy-start | bytes 9220
  2.2 1.2 %copy-start.2 = (bf16[1024,128]{1,0:T(8,128)(2,1)S(1)}, bf16[1024,128]{1,0:T(8,128)(2,1)}, u32[]{:S(2)}) copy-start(bf16[1024,128]{1,0:T(8,128)(2,1)} %w_b.1) | copy-start | bytes 786436
  2.2 1.2 %copy-start.3 = (bf16[1024,128]{1,0:T(8,128)(2,1)S(1)}, bf16[1024,128]{1,0:T(8,128)(2,1)}, u32[]{:S(2)}) copy-start(bf16[1024,128]{1,0:T(8,128)(2,1)} %w_c.1) | copy-start | bytes 786436
  2.2 1.2 %copy-start.6 = (bf16[1,8,2048]{2,1,0:T(8,128)(2,1)S(1)}, bf16[1,8,2048]{2,1,0:T(8,128)(2,1)}, u32[]{:S(2)}) copy-start(bf16[1,8,2048]{2,1,0:T(8,128)(2,1)} %context.1) | copy-start | bytes 98308
  3.4 1.2 %copy-start = (bf16[1024,512]{1,0:T(8,128)(2,1)S(1)}, bf16[1024,512]{1,0:T(8,128)(2,1)}, u32[]{:S(2)}) copy-start(bf16[1024,512]{1,0:T(8,128)(2,1)} %w_x.1) | copy-start | bytes 3145732
  4.6 1.2 %copy-start.1 = (bf16[1024,512]{1,0:T(8,128)(2,1)S(1)}, bf16[1024,512]{1,0:T(8,128)(2,1)}, u32[]{:S(2)}) copy-start(bf16[1024,512]{1,0:T(8,128)(2,1)} %w_z.1) | copy-start | bytes 3145732
  5.8 0.9 %copy-start.4 = (bf16[1,32,2048]{2,1,0:T(8,128)(2,1)S(1)}, bf16[1,32,2048]{2,1,0:T(8,128)(2,1)}, u32[]{:S(2)}) copy-start(bf16[1,32,2048]{2,1,0:T(8,128)(2,1)} %latent.1) | copy-start | bytes 393220
  6.7 0.9 %copy-start.5 = (bf16[3,32,512]{2,1,0:T(8,128)(2,1)S(1)}, bf16[3,32,512]{2,1,0:T(8,128)(2,1)}, u32[]{:S(2)}) copy-start(bf16[3,32,512]{2,1,0:T(8,128)(2,1)} %mod_w.1) | copy-start | bytes 294916

commit v2 on v1

--- a/solution.py
+++ b/solution.py
@@ -80,10 +80,12 @@
     v_tb,
     v_tc,
     v_rate,
+    v_rates,
     v_og,
     v_wo,
     v_p,
     v_my,
+    v_pz,
     v_mz,
     v_ms,
     v_mx,
@@ -128,19 +130,32 @@
     c = lax.axis_index("dp")
     k = z * NY + y
 
-    barrier = pltpu.get_barrier_semaphore()
+    def along_y(d):
+        return {"sp_1": lax.rem(y + d, NY)}
+
+    def along_z(d):
+        return {"sp_0": lax.rem(z + d, NZ)}
+
+    def along_x(d):
+        return {"tp": lax.rem(t + d, TP)}
+
     after = lax.rem(k + 1, NSP)
     before = lax.rem(k + NSP - 1, NSP)
-    after_id = {"sp_0": after // NY, "sp_1": lax.rem(after, NY)}
-    before_id = {"sp_0": before // NY, "sp_1": lax.rem(before, NY)}
+    partner = {"dp": 1 - c}
+
+    def beside(place, d):
+        return {"sp_0": place // NY, "sp_1": lax.rem(place, NY), "tp": jnp.int32(d)}
+
+    barrier = pltpu.get_barrier_semaphore()
     for d in (4, 3, 5, 2, 6, 1, 7):
-        pl.semaphore_signal(barrier, 1, device_id={"sp_1": lax.rem(y + d, NY)}, device_id_type=MESH)
-        pl.semaphore_signal(barrier, 1, device_id={"sp_0": lax.rem(z + d, NZ)}, device_id_type=MESH)
+        pl.semaphore_signal(barrier, 1, device_id=along_y(d), device_id_type=MESH)
+        pl.semaphore_signal(barrier, 1, device_id=along_z(d), device_id_type=MESH)
     for d in (2, 1, 3):
-        pl.semaphore_signal(barrier, 1, device_id={"tp": lax.rem(t + d, TP)}, device_id_type=MESH)
-    pl.semaphore_signal(barrier, 1, device_id={"dp": 1 - c}, device_id_type=MESH)
-    pl.semaphore_signal(barrier, 1, device_id=after_id, device_id_type=MESH)
-    pl.semaphore_signal(barrier, 1, device_id=before_id, device_id_type=MESH)
+        pl.semaphore_signal(barrier, 1, device_id=along_x(d), device_id_type=MESH)
+    pl.semaphore_signal(barrier, 1, device_id=partner, device_id_type=MESH)
+    for d in range(TP):
+        pl.semaphore_signal(barrier, 1, device_id=beside(after, d), device_id_type=MESH)
+        pl.semaphore_signal(barrier, 1, device_id=beside(before, d), device_id_type=MESH)
 
     half = pl.ds(pl.multiple_of(c * 1024, 1024), 1024)
     whalf = pl.ds(pl.multiple_of(c * 256, 256), 256)
@@ -158,7 +173,7 @@
         (out_gain, v_og),
     ]
     weights = [
-        (w_dt, v_dt.at[:, half, :]),
+        (w_dt, v_dt.at[:, :, half]),
         (w_b, v_w.at[2, half, 0:128]),
         (w_c, v_w.at[2, half, 128:256]),
         (w_x.at[:, 0:256], v_w.at[0, half, :]),
@@ -173,8 +188,6 @@
     for copy in local:
         copy.start()
 
-    pl.semaphore_wait(barrier, 20)
-
     def remote(a, b, ssem, rsem, where):
         return pltpu.make_async_remote_copy(
             src_ref=a, dst_ref=b, send_sem=ssem, recv_sem=rsem, device_id=where, device_id_type=MESH
@@ -186,12 +199,13 @@
     lane0 = pl.ds(pl.multiple_of((k // 4) * 128, 128), 128)
     shift = lax.rem(128 - lax.rem(k, 4) * 32, 128)
 
-    def own_act(ref):
-        act = silu(ref[0:1, lane0].astype(F32)).astype(BF16).astype(F32)
+    def own_act(values):
+        act = silu(values).astype(BF16).astype(F32)
         return pltpu.roll(jnp.broadcast_to(act, (8, 128)), shift, 1)
 
-    act_lat = own_act(v_cond)
-    act_ctx = own_act(v_src)
+    src_rows = jnp.where(iota((16, 128), 0) == k // 4, v_src[...].astype(F32), 0.0)
+    act_lat = own_act(v_cond[0:1, lane0].astype(F32))
+    act_ctx = own_act(jnp.sum(src_rows, axis=0, keepdims=True))
     row8 = iota((8, 128), 0)
     zero8 = jnp.zeros((8, 128), F32)
     lhs = (
@@ -200,30 +214,50 @@
         jnp.where(row8 == 2, act_lat, zero8),
     )
     partial = sum(dot(lhs[i][:, 0:32].astype(BF16), v_mod[i]) for i in range(3))
-    v_p[...] = partial
-
-    def exchange(src, slots, axis, me, peers, ssem, rsem):
-        order = sorted(range(1, peers), key=lambda d: -min(d, peers - d))
+    v_p[...] = partial.astype(BF16)
+    pl.semaphore_wait(barrier, 26)
+
+    def exchange(src, slots, along, ssem, rsem):
         copies = [
-            remote(src, slots.at[d], ssem.at[d], rsem.at[d], {axis: lax.rem(me + d, peers)})
-            for d in order
+            remote(src, slots.at[d], ssem.at[d], rsem.at[d], along(d))
+            for d in (4, 3, 5, 2, 6, 1, 7)
         ]
         for copy in copies:
             copy.start()
         return copies
 
-    y_copies = exchange(v_p, v_my, "sp_1", y, NY, ys_sem, yr_sem)
+    y_copies = exchange(v_p, v_my, along_y, ys_sem, yr_sem)
+
+    local[3].wait()
+    v_edge[0] = v_lat[t, 0:8, :].astype(F32)[0:1]
+    v_edge[1] = v_lat[t, 24:32, :].astype(F32)[7:8]
+    last_copies = [
+        remote(v_edge.at[1], v_halo.at[0], hs_sem.at[0, d], hr_sem.at[0], beside(after, d))
+        for d in range(TP)
+    ]
+    first_copies = [
+        remote(v_edge.at[0], v_halo.at[1], hs_sem.at[1, d], hr_sem.at[1], beside(before, d))
+        for d in range(TP)
+    ]
+
+    @pl.when(t == TP - 1)
+    def _():
+        for copy in last_copies:
+            copy.start()
+
+    @pl.when(t == 0)
+    def _():
+        for copy in first_copies:
+            copy.start()
 
     lat_copies = [
-        remote(
-            latent.at[0], v_lat.at[t], ls_sem.at[d], lr_sem.at[d], {"tp": lax.rem(t + d, TP)}
-        )
+        remote(latent.at[0], v_lat.at[t], ls_sem.at[d], lr_sem.at[d], along_x(d))
         for d in (2, 1, 3)
     ]
     for copy in lat_copies:
         copy.start()
     w_copies = [
-        remote(a, b, ws_sem.at[i], wr_sem.at[i], {"dp": 1 - c}) for i, (a, b) in enumerate(weights)
+        remote(a, b, ws_sem.at[i], wr_sem.at[i], partner) for i, (a, b) in enumerate(weights)
     ]
     for copy in w_copies:
         copy.start()
@@ -235,55 +269,53 @@
     )
     v_e[...] = jnp.where(hit, 1.0, 0.0).astype(BF16)
     v_pdt[...] = jnp.zeros((M, 128), F32)
+    local[9].wait()
+    v_rates[...] = jnp.zeros((1, 128), F32)
+    v_rates[0:1, 0:8] = v_rate[0:1]
+    v_rates[0:1, 8:16] = v_rate[1:2]
+
+    def inverse(rows):
+        return lax.rsqrt(jnp.mean(rows * rows, axis=-1, keepdims=True) + EPS)
 
     for copy in y_copies:
         copy.wait_recv()
-    v_ms[0] = v_p[...] + sum(v_my[d] for d in range(1, NY))
-    z_copies = exchange(v_ms.at[0], v_mz, "sp_0", z, NZ, zs_sem, zr_sem)
-
-    local[3].wait()
-    for copy in lat_copies:
-        copy.wait_recv()
-    v_edge[0] = v_lat[0, 0:8, :].astype(F32)[0:1]
-    v_edge[1] = v_lat[TP - 1, 24:32, :].astype(F32)[7:8]
-    last_copy = remote(v_edge.at[1], v_halo.at[0], hs_sem.at[0], hr_sem.at[0], after_id)
-    first_copy = remote(v_edge.at[0], v_halo.at[1], hs_sem.at[1], hr_sem.at[1], before_id)
-    last_copy.start()
-    first_copy.start()
-
-    def inverse(rows):
-        return lax.rsqrt(jnp.mean(rows * rows, axis=-1, keepdims=True) + EPS)
-
-    inv_lat = [inverse(v_lat[i].astype(F32)) for i in range(TP)]
-
-    for copy in z_copies:
-        copy.wait_recv()
-    v_ms[1] = v_ms[0] + sum(v_mz[d] for d in range(1, NZ))
-    v_mx[t] = v_ms[1]
-    x_copies = [
-        remote(v_ms.at[1], v_mx.at[t], xs_sem.at[d], xr_sem.at[d], {"tp": lax.rem(t + d, TP)})
-        for d in (2, 1, 3)
-    ]
-    for copy in x_copies:
-        copy.start()
+    z_sum = v_p[...].astype(F32) + sum(v_my[d].astype(F32) for d in range(1, NY))
+    v_pz[...] = z_sum.astype(BF16)
+    z_copies = exchange(v_pz, v_mz, along_z, zs_sem, zr_sem)
+
     for i in range(4, len(local)):
-        local[i].wait()
+        if i != 9:
+            local[i].wait()
     ctx_rows = v_ctx[...].astype(F32)
     inv_ctx = inverse(ctx_rows)
-    last_copy.wait_recv()
-    first_copy.wait_recv()
+    last_copies[0].wait_recv()
+    first_copies[0].wait_recv()
     row_h = iota((8, D), 0)
     halo = jnp.where(row_h == 0, v_halo[0], jnp.where(row_h == 1, v_halo[1], jnp.zeros((8, D), F32)))
     inv_halo = inverse(halo)
+
+    for copy in z_copies:
+        copy.wait_recv()
+    v_ms[...] = z_sum + sum(v_mz[d].astype(F32) for d in range(1, NZ))
+    v_mx[t] = v_ms[...]
+    x_copies = [
+        remote(v_ms, v_mx.at[t], xs_sem.at[d], xr_sem.at[d], along_x(d)) for d in (2, 1, 3)
+    ]
+    for copy in x_copies:
+        copy.start()
+    for copy in lat_copies:
+        copy.wait_recv()
+    inv_lat = [inverse(v_lat[i].astype(F32)) for i in range(TP)]
     for copy in w_copies:
         copy.wait_recv()
     for copy in x_copies:
         copy.wait_recv()
 
+    gains = v_gain[...].astype(F32)
     for j in range(TP):
         cols = slice(j * 512, (j + 1) * 512)
         mods = v_mx[j]
-        gain_j = v_gain[0:1, cols].astype(F32)
+        gain_j = jnp.concatenate([gains[4 * j + i : 4 * j + i + 1] for i in range(4)], axis=1)
         mul = gain_j * (1.0 + mods[1:2])
         add = mods[0:1]
         for i in range(TP):
@@ -293,8 +325,9 @@
         halo_h = halo[:, cols] * inv_halo * mul + add
         v_h[TOK:M, cols] = jnp.concatenate([ctx_h, halo_h], axis=0).astype(BF16)
 
-    v_pdt[:, 0:8] = dot(v_h[...], v_dt[0])
-    v_pdt[:, 8:16] = dot(v_h[...], v_dt[1])
+    v_pdt[:, 0:16] = lax.dot_general(
+        v_h[...], v_dt[...].reshape(16, D), (((1,), (1,)), ((), ())), preferred_element_type=F32
+    )
     for i in (2, 0, 1):
         v_f[i] = dot(v_h[...], v_w[i])
 
@@ -302,7 +335,7 @@
     row = iota((TOK, 128), 0)
     lane8 = iota((8, 128), 1)
     lane16 = iota((16, 128), 1)
-    rate = v_rate[...]
+    rate = v_rates[...]
     step = softplus(v_pdt[0:TOK])
     decay = -rate * step
     parts = high_low(decay, 16)
@@ -328,38 +361,32 @@
             tile = jnp.where(lane8 < 64, x_tile, jnp.where(lane8 < 80, b_tiles[n], tail))
             v_cts[h * 8 + n] = tile.astype(BF16)
 
-    def place(i):
-        a = i // 8
-        b = lax.rem(i, 8)
-
-        def offset(v):
-            halved = (v + 1) // 2
-            return jnp.where(lax.rem(v, 2) == 1, 4 - halved, 4 + halved)
-
-        z_to = lax.rem(z + offset(a), NZ)
-        y_to = lax.rem(y + offset(b), NY)
-        return z_to, y_to
+    y_places = [lax.rem(y + d, NY) for d in range(NY)]
+    near = (4, 3, 5, 2, 6, 1, 7, 0)
 
     def all_to_all(src, dst, base):
-        def send(i, carry):
-            z_to, y_to = place(i)
-            remote(
-                src.at[z_to * NY + y_to],
-                dst.at[k],
-                a_sem.at[base],
-                a_sem.at[base + 1],
-                {"sp_0": z_to, "sp_1": y_to},
-            ).start()
+        def send(z_to, d):
+            to = z_to * NY + y_places[d]
+            remote(src.at[to], dst.at[k], a_sem.at[base], a_sem.at[base + 1], {"sp_0": z_to, "sp_1": y_places[d]}).start()
+
+        def send_row(i, carry):
+            half_i = (i + 1) // 2
+            off = jnp.where(lax.rem(i, 2) == 1, 4 - half_i, 4 + half_i)
+            z_to = lax.rem(z + off, NZ)
+            for d in near:
+                send(z_to, d)
             return carry
 
-        lax.fori_loop(0, NSP - 1, send, 0)
+        lax.fori_loop(0, NZ - 1, send_row, 0)
+        for d in near[:-1]:
+            send(z, d)
         dst[k] = src[k]
         return remote(
             src.at[pl.ds(0, NSP - 1)],
             dst.at[pl.ds(0, NSP - 1)],
             a_sem.at[base],
             a_sem.at[base + 1],
-            after_id,
+            partner,
         )
 
     ctx_wait = all_to_all(v_cts, v_ctr, 0)
@@ -495,7 +522,7 @@
     inv = lax.rsqrt(squares / 512.0 + EPS)
     for p in range(4):
         cols = slice(p * 128, (p + 1) * 128)
-        v_ny[:, cols] = (gated[p] * inv * v_og[0:1, cols].astype(F32)).astype(BF16)
+        v_ny[:, cols] = (gated[p] * inv * v_og[...].astype(F32)[p : p + 1]).astype(BF16)
 
     out_copies = []
     for n in range(2):
@@ -507,7 +534,7 @@
         for d in (2, 1, 3):
             to = lax.rem(t + d, TP)
             copy = remote(
-                v_po.at[n, to], v_pr.at[n, d], p_ssem.at[n, d], p_rsem.at[n, d], {"tp": to}
+                v_po.at[n, to], v_pr.at[n, d], p_ssem.at[n, d], p_rsem.at[n, d], along_x(d)
             )
             copy.start()
             out_copies.append(copy)
@@ -522,10 +549,19 @@
             j = n * 2 + q
             out[0, :, j * 512 : (j + 1) * 512] = (v_mx[j, 2:3] * mixed).astype(BF16)
 
-    for copy in (
-        y_copies + z_copies + x_copies + lat_copies + w_copies + [last_copy, first_copy] + out_copies
-    ):
+    for copy in y_copies + z_copies + x_copies + lat_copies + w_copies + out_copies:
         copy.wait_send()
+
+    @pl.when(t == TP - 1)
+    def _():
+        for copy in last_copies:
+            copy.wait_send()
+
+    @pl.when(t == 0)
+    def _():
+        for copy in first_copies:
+            copy.wait_send()
+
     ctx_wait.wait_send()
     state_wait.wait_send()
     back_wait.wait_send()
@@ -550,28 +586,29 @@
     out_gain,
     w_out,
 ):
-    rates = jnp.pad(decay_rate.reshape(1, 16), ((0, 0), (0, 112)))
     dma = pltpu.SemaphoreType.DMA
     vmem = pltpu.VMEM
     scratch = [
         vmem((TP, ROWS, D), BF16),
         vmem((1, D), BF16),
         vmem((CTXR, D), BF16),
-        vmem((1, D), BF16),
+        vmem((16, 128), BF16),
         vmem((3, 32, 512), BF16),
-        vmem((1, D), BF16),
+        vmem((16, 128), BF16),
         vmem((5, D, 256), BF16),
-        vmem((2, D, 8), BF16),
+        vmem((2, 8, D), BF16),
         vmem((3, 512), BF16),
         vmem((3, 128), BF16),
         vmem((3, 128), BF16),
+        vmem((2, 8), F32),
         vmem((1, 128), F32),
-        vmem((1, 512), BF16),
+        vmem((4, 128), BF16),
         vmem((512, D), BF16),
+        vmem((8, 512), BF16),
+        vmem((NY, 8, 512), BF16),
+        vmem((8, 512), BF16),
+        vmem((NZ, 8, 512), BF16),
         vmem((8, 512), F32),
-        vmem((NY, 8, 512), F32),
-        vmem((NZ, 8, 512), F32),
-        vmem((2, 8, 512), F32),
         vmem((TP, 8, 512), F32),
         vmem((2, 1, D), F32),
         vmem((2, 1, D), F32),
@@ -602,7 +639,7 @@
         dma((NZ,)),
         dma((TP,)),
         dma((TP,)),
-        dma((2,)),
+        dma((2, TP)),
         dma((2,)),
         dma((6,)),
         dma((2, TP)),
@@ -610,12 +647,12 @@
     ]
     call = pl.pallas_call(
         kernel,
-        out_shape=jax.ShapeDtypeStruct((1, ROWS, D), BF16),
-        in_specs=[pl.BlockSpec(memory_space=pl.ANY)] * 17,
+        out_shape=pltpu.VMEM((1, ROWS, D), BF16),
+        in_specs=[pl.BlockSpec(memory_space=pltpu.HBM)] * 17,
         out_specs=pl.BlockSpec(memory_space=pltpu.VMEM),
         scratch_shapes=scratch,
         compiler_params=pltpu.CompilerParams(
-            collective_id=0, has_side_effects=True, vmem_limit_bytes=50 * 1024 * 1024
+            collective_id=0, has_side_effects=True, vmem_limit_bytes=66900000
         ),
         name="mixer",
     )
@@ -623,19 +660,19 @@
         latent,
         condition,
         context,
-        context_source.reshape(1, D),
+        context_source.reshape(16, 128),
         mod_weight,
-        norm_gain.reshape(1, D),
+        norm_gain.reshape(16, 128),
         w_x,
         w_b,
         w_c,
         w_z,
-        w_dt,
+        jnp.swapaxes(w_dt, 1, 2),
         conv_x,
         conv_b,
         conv_c,
-        rates,
-        out_gain.reshape(1, 512),
+        decay_rate,
+        out_gain.reshape(4, 128),
         w_out,
     )
 

time: 66.2 us -> 54.2 us (0.82)
  the two profiles are of different devices: /device:TPU:1 before, /device:TPU:8 now
where the time goes in v2:
time: 54.2 us; the launch traced here: 54.1 us
  Pallas kernels  53.4 us (99%)
  local copies, waits for them, and re-layouts  0.66 us (1%)
    pallas_call x1, Pallas kernels, shards(): call(latent, condition, context, context_source.reshape(16, 128), mod_wei...  53.4 us

profile of v2, /device:TPU:8, one launch (start us, length us, event | category | flops | bytes accessed | tf_op | source)
XLA Modules:
  0.0 54.1 jit_solution(4615566156081720944)
XLA Ops:
  0.0 53.4 %mixer.1 = bf16[1,32,2048]{2,1,0:T(8,128)(2,1)S(1)} custom-call(bf16[1,32,2048]{2,1,0:T(8,128)(2,1)} %latent.1, bf16[1,2048]{1,0:T(2,128)(2,1)} %condition.1, bf16[1,8,2048]{2,1,0:T(8,128)(2,1)} %context.1, bf16[16,128]{1,0:T(8,128)(2,1)} %bitcast.5, bf16[3,32,512]{2,1,0:T(8,128)(2,1)} %mod_w.1, bf16[16,128]{1,0:T(8,128)(2,1)} %bitcast.6, ...), custom_call_target="tpu_custom_call" | custom-call | tf_op jit(solution)/shard_map/mixer/pallas_call | solution.py:659
  53.4 0.7 %copy.19 = bf16[1,32,2048]{2,1,0:T(8,128)(2,1)} copy(bf16[1,32,2048]{2,1,0:T(8,128)(2,1)S(1)} %mixer.1) | data formatting | bytes 262144

commit v3 on v2

--- a/solution.py
+++ b/solution.py
@@ -103,6 +103,8 @@
     v_t,
     v_o,
     v_hin,
+    v_xin,
+    v_g,
     v_y,
     v_ny,
     v_po,
@@ -120,7 +122,10 @@
     xr_sem,
     hs_sem,
     hr_sem,
-    a_sem,
+    as_sem,
+    ar_sem,
+    bs_sem,
+    br_sem,
     p_ssem,
     p_rsem,
 ):
@@ -145,17 +150,6 @@
 
     def beside(place, d):
         return {"sp_0": place // NY, "sp_1": lax.rem(place, NY), "tp": jnp.int32(d)}
-
-    barrier = pltpu.get_barrier_semaphore()
-    for d in (4, 3, 5, 2, 6, 1, 7):
-        pl.semaphore_signal(barrier, 1, device_id=along_y(d), device_id_type=MESH)
-        pl.semaphore_signal(barrier, 1, device_id=along_z(d), device_id_type=MESH)
-    for d in (2, 1, 3):
-        pl.semaphore_signal(barrier, 1, device_id=along_x(d), device_id_type=MESH)
-    pl.semaphore_signal(barrier, 1, device_id=partner, device_id_type=MESH)
-    for d in range(TP):
-        pl.semaphore_signal(barrier, 1, device_id=beside(after, d), device_id_type=MESH)
-        pl.semaphore_signal(barrier, 1, device_id=beside(before, d), device_id_type=MESH)
 
     half = pl.ds(pl.multiple_of(c * 1024, 1024), 1024)
     whalf = pl.ds(pl.multiple_of(c * 256, 256), 256)
@@ -185,7 +179,25 @@
     local = [
         pltpu.make_async_copy(a, b, loc_sem.at[i]) for i, (a, b) in enumerate(small + weights)
     ]
-    for copy in local:
+    for copy in local[0:4]:
+        copy.start()
+
+    barrier = pltpu.get_barrier_semaphore()
+
+    def greet(where):
+        pl.semaphore_signal(barrier, 1, device_id=where, device_id_type=MESH)
+
+    for d in (4, 3, 5, 2, 6, 1, 7):
+        greet(along_y(d))
+        greet(along_z(d))
+        if d == 4:
+            greet(beside(before, TP - 1))
+            greet(beside(after, 0))
+    for d in (2, 1, 3):
+        greet(along_x(d))
+    greet(partner)
+
+    for copy in local[4:]:
         copy.start()
 
     def remote(a, b, ssem, rsem, where):
@@ -215,7 +227,7 @@
     )
     partial = sum(dot(lhs[i][:, 0:32].astype(BF16), v_mod[i]) for i in range(3))
     v_p[...] = partial.astype(BF16)
-    pl.semaphore_wait(barrier, 26)
+    pl.semaphore_wait(barrier, 18 + jnp.where((t == 0) | (t == TP - 1), 4, 0))
 
     def exchange(src, slots, along, ssem, rsem):
         copies = [
@@ -353,43 +365,43 @@
     tail = pltpu.roll(tail, 80, 1)
     ctx_b = v_f[2, TOK : TOK + 8, 0:128]
     b_tiles = [pltpu.roll(ctx_b, (64 - 16 * n) % 128, 1) for n in range(8)]
-    for h in range(8):
-        x_tile = v_f[h // 4, TOK : TOK + 8, ((h // 2) % 2) * 128 : ((h // 2) % 2) * 128 + 128]
-        if h % 2:
-            x_tile = pltpu.roll(x_tile, 64, 1)
+    y_places = [lax.rem(y + d, NY) for d in range(NY)]
+    near = (4, 3, 5, 2, 6, 1, 7, 0)
+
+    def to_owners(make, groups, src, dst, which):
+        for group in groups:
+            rows = [lax.rem(z + d, NZ) for d in group]
+            for h in rows:
+                make(h)
+            for d_z, h in zip(group, rows, strict=True):
+                for d in near if d_z else near[:-1]:
+                    remote(
+                        src.at[h * NY + y_places[d]],
+                        dst.at[c, k],
+                        as_sem.at[which],
+                        ar_sem.at[which, c],
+                        {"sp_0": h, "sp_1": y_places[d], "dp": 1},
+                    ).start()
+
+        @pl.when(c == 0)
+        def _():
+            remote(src.at[k], dst.at[0, k], as_sem.at[which], ar_sem.at[which, 0], partner).start()
+
+        @pl.when(c == 1)
+        def _():
+            dst[1, k] = src[k]
+
+    def whole(src, dst, count, ssem, rsem):
+        return remote(src.at[pl.ds(0, count)], dst.at[pl.ds(0, count)], ssem, rsem, partner)
+
+    def context_tiles(h):
+        x_tile = v_f[h // 4, TOK : TOK + 8, pl.ds(pl.multiple_of(lax.rem(h // 2, 2) * 128, 128), 128)]
+        x_tile = jnp.where(lax.rem(h, 2) == 0, x_tile, pltpu.roll(x_tile, 64, 1))
         for n in range(8):
             tile = jnp.where(lane8 < 64, x_tile, jnp.where(lane8 < 80, b_tiles[n], tail))
             v_cts[h * 8 + n] = tile.astype(BF16)
 
-    y_places = [lax.rem(y + d, NY) for d in range(NY)]
-    near = (4, 3, 5, 2, 6, 1, 7, 0)
-
-    def all_to_all(src, dst, base):
-        def send(z_to, d):
-            to = z_to * NY + y_places[d]
-            remote(src.at[to], dst.at[k], a_sem.at[base], a_sem.at[base + 1], {"sp_0": z_to, "sp_1": y_places[d]}).start()
-
-        def send_row(i, carry):
-            half_i = (i + 1) // 2
-            off = jnp.where(lax.rem(i, 2) == 1, 4 - half_i, 4 + half_i)
-            z_to = lax.rem(z + off, NZ)
-            for d in near:
-                send(z_to, d)
-            return carry
-
-        lax.fori_loop(0, NZ - 1, send_row, 0)
-        for d in near[:-1]:
-            send(z, d)
-        dst[k] = src[k]
-        return remote(
-            src.at[pl.ds(0, NSP - 1)],
-            dst.at[pl.ds(0, NSP - 1)],
-            a_sem.at[base],
-            a_sem.at[base + 1],
-            partner,
-        )
-
-    ctx_wait = all_to_all(v_cts, v_ctr, 0)
+    to_owners(context_tiles, (near,), v_cts, v_ctr, 0)
 
     has_before = jnp.where(k > 0, 1.0, 0.0)
     has_after = jnp.where(k < NSP - 1, 1.0, 0.0)
@@ -405,21 +417,23 @@
         return silu(down * w[0:1] + block * w[1:2] + up * w[2:3])
 
     b_in = conv(2, 0, v_tb[...]).astype(BF16)
-    x_in = [conv(p // 2, (p % 2) * 128, v_tx[:, p * 128 : (p + 1) * 128]) for p in range(4)]
+    for p in range(4):
+        v_xin[p] = conv(p // 2, (p % 2) * 128, v_tx[:, p * 128 : (p + 1) * 128])
     b_turned = b_in.astype(F32).T.astype(BF16)
 
     to_end = jnp.where(lane < 16, step * jnp.exp(total - cum), 0.0)
     moved = high_low(to_end, 16)[:, 0:32]
-    for p in range(4):
-        turned = pltpu.roll(x_in[p], 64, 1)
-        for s in range(2):
-            h = 2 * p + s
-            pair = jnp.where(lane < 64, x_in[p], turned) if s == 0 else jnp.where(lane < 64, turned, x_in[p])
-            scaled = (pair * dot(moved, v_e[:, h * 128 : (h + 1) * 128])).astype(BF16)
-            state = dot(b_turned, scaled).astype(BF16)
-            for n in range(8):
-                v_s[h * 8 + n] = state[n * 16 : (n + 1) * 16]
-    state_wait = all_to_all(v_s, v_r, 2)
+    lane_side = lax.shift_right_logical(lane, 6)
+
+    def state_tiles(h):
+        x_pair = v_xin[h // 2]
+        doubled = jnp.where(lane_side == lax.rem(h, 2), x_pair, pltpu.roll(x_pair, 64, 1))
+        coefs = dot(moved, v_e[:, pl.ds(pl.multiple_of(h * 128, 128), 128)])
+        state = dot(b_turned, (doubled * coefs).astype(BF16)).astype(BF16)
+        for n in range(8):
+            v_s[h * 8 + n] = state[n * 16 : (n + 1) * 16]
+
+    to_owners(state_tiles, (near[:4], near[4:]), v_s, v_r, 1)
 
     for i in (3, 4):
         v_f[i] = dot(v_h[...], v_w[i])
@@ -428,7 +442,7 @@
     step_t = step.T
     cum_t = cum.T
     for p in range(4):
-        x_pair = x_in[p].astype(BF16)
+        x_pair = v_xin[p].astype(BF16)
         sides = []
         for s in range(2):
             h = 2 * p + s
@@ -444,9 +458,12 @@
             sides.append(dot(weight.astype(BF16), x_pair))
         v_y[p] = jnp.where(lane < 64, sides[0], sides[1])
     growth = high_low(jnp.where(lane < 16, jnp.exp(cum), 0.0), 16)[:, 0:32]
-
-    ctx_wait.wait_recv()
-    feats = v_ctr[...].astype(F32).reshape(NSP * CTXR, 128)
+    for h in range(8):
+        v_g[h] = dot(growth, v_e[:, h * 128 : (h + 1) * 128])
+    for p in range(4):
+        cols = slice((p % 2) * 128, (p % 2) * 128 + 128)
+        v_f[3 + p // 2, 0:TOK, cols] = silu(v_f[3 + p // 2, 0:TOK, cols])
+
     row_c = iota((NSP * CTXR, 128), 0)
     lane_c = iota((NSP * CTXR, 128), 1)
     x_lanes = pl.ds(pl.multiple_of((z // 2) * 128, 128), 128)
@@ -458,54 +475,81 @@
         tb = jnp.broadcast_to(v_tb[i : i + 1].astype(F32), (8, 128))
         return jnp.where(lane8 < 64, pltpu.roll(tx, x_shift, 1), pltpu.roll(tb, b_shift, 1))[0:1]
 
-    down = jnp.where(row_c == 0, 0.0, pltpu.roll(feats, 1, 0))
-    up = jnp.where(row_c == NSP * CTXR - 1, 0.0, pltpu.roll(feats, NSP * CTXR - 1, 0))
-    smooth = silu(down * owner_tap(0) + feats * owner_tap(1) + up * owner_tap(2))
-    picked = pltpu.roll(feats, lax.rem(128 - z, 128), 1)
-    used = (lane_c == 80) | (lane_c == 88)
-    step_c = softplus(picked)
-    rate_c = pltpu.roll(jnp.broadcast_to(rate, (8, 128)), 80 - z, 1)[0:1]
-    decay_c = jnp.where(used, -rate_c * step_c, 0.0)
-    parts_c = high_low(decay_c, 1)
-    run = jnp.zeros((1, 128), F32)
-    pieces = []
-    for b in range(4):
-        piece = dot(lower, parts_c[b * 128 : (b + 1) * 128]) + run
-        run = piece[127:128]
-        pieces.append(piece)
-    prefix = jnp.concatenate(pieces, axis=0)
-    prefix = prefix + pltpu.roll(prefix, 127, 1)
-    end = prefix[NSP * CTXR - 1 :]
-    reach = jnp.where(lane_c < 84, end - prefix, prefix - decay_c)
-    weight_c = jnp.where(used, step_c * jnp.exp(jnp.where(used, reach, 0.0)), 0.0)
-    smooth = smooth.astype(BF16)
-    x_wide = smooth.astype(F32)
-    spread_x = jnp.where(
-        lane_c < 64, x_wide * weight_c[:, 80:81], pltpu.roll(x_wide, 64, 1) * weight_c[:, 88:89]
-    )
-    context_state = tdot(smooth, spread_x.astype(BF16))[64:80]
-    grow = jnp.exp(jnp.where((lane_c >= 96) & (lane_c < 112), picked + pltpu.roll(picked, 112, 1), 0.0))
-    v_dec[...] = jnp.where(lane_c < 64, grow[:, 96:97], grow[:, 104:105]).reshape(NSP, 8, 128)
-
-    state_wait.wait_recv()
-
-    def advance(i, carry):
-        j = NSP - 1 - i
-        v_t[i] = carry
-        new = jnp.where(lane16 < 64, v_r[i].astype(F32), v_r[j].astype(F32))
-        scale = jnp.where(lane8 < 64, v_dec[i], v_dec[j])
-        return carry * jnp.concatenate([scale, scale], axis=0) + new
-
-    lax.fori_loop(0, NSP, advance, context_state, unroll=8)
-
-    def collect(i, carry):
-        v_o[i] = jnp.where(lane16 < 64, v_t[i], v_t[NSP - 1 - i]).astype(BF16)
-        return carry
-
-    lax.fori_loop(0, NSP, collect, 0, unroll=8)
-    back_wait = all_to_all(v_o, v_hin, 4)
-
-    back_wait.wait_recv()
+    def own_part(sample):
+        count = NSP if sample == 0 else NSP - 1
+        whole(v_cts, v_ctr.at[sample], count, as_sem.at[0], ar_sem.at[0, sample]).wait_recv()
+        feats = v_ctr[sample].astype(F32).reshape(NSP * CTXR, 128)
+        down = jnp.where(row_c == 0, 0.0, pltpu.roll(feats, 1, 0))
+        up = jnp.where(row_c == NSP * CTXR - 1, 0.0, pltpu.roll(feats, NSP * CTXR - 1, 0))
+        smooth = silu(down * owner_tap(0) + feats * owner_tap(1) + up * owner_tap(2))
+        picked = pltpu.roll(feats, lax.rem(128 - z, 128), 1)
+        used = (lane_c == 80) | (lane_c == 88)
+        step_c = softplus(picked)
+        rate_c = pltpu.roll(jnp.broadcast_to(rate, (8, 128)), 80 - z, 1)[0:1]
+        decay_c = jnp.where(used, -rate_c * step_c, 0.0)
+        parts_c = high_low(decay_c, 1)
+        run = jnp.zeros((1, 128), F32)
+        pieces = []
+        for b in range(4):
+            piece = dot(lower, parts_c[b * 128 : (b + 1) * 128]) + run
+            run = piece[127:128]
+            pieces.append(piece)
+        prefix = jnp.concatenate(pieces, axis=0)
+        prefix = prefix + pltpu.roll(prefix, 127, 1)
+        end = prefix[NSP * CTXR - 1 :]
+        reach = jnp.where(lane_c < 84, end - prefix, prefix - decay_c)
+        weight_c = jnp.where(used, step_c * jnp.exp(jnp.where(used, reach, 0.0)), 0.0)
+        smooth = smooth.astype(BF16)
+        x_wide = smooth.astype(F32)
+        spread_x = jnp.where(
+            lane_c < 64, x_wide * weight_c[:, 80:81], pltpu.roll(x_wide, 64, 1) * weight_c[:, 88:89]
+        )
+        context_state = tdot(smooth, spread_x.astype(BF16))[64:80]
+        grow = jnp.exp(jnp.where((lane_c >= 96) & (lane_c < 112), picked + pltpu.roll(picked, 112, 1), 0.0))
+        v_dec[...] = jnp.where(lane_c < 64, grow[:, 96:97], grow[:, 104:105]).reshape(NSP, 8, 128)
+
+        whole(v_s, v_r.at[sample], count, as_sem.at[1], ar_sem.at[1, sample]).wait_recv()
+
+        def advance(i, carry):
+            j = NSP - 1 - i
+            v_t[i] = carry
+            new = jnp.where(lane16 < 64, v_r[sample, i].astype(F32), v_r[sample, j].astype(F32))
+            scale = jnp.where(lane8 < 64, v_dec[i], v_dec[j])
+            return carry * jnp.concatenate([scale, scale], axis=0) + new
+
+        lax.fori_loop(0, NSP, advance, context_state, unroll=8)
+
+        def collect(i, carry):
+            v_o[sample, i] = jnp.where(lane16 < 64, v_t[i], v_t[NSP - 1 - i]).astype(BF16)
+            return carry
+
+        lax.fori_loop(0, NSP, collect, 0, unroll=8)
+        for d_z in near:
+            z_to = lax.rem(z + d_z, NZ)
+            for d in near if d_z or sample == 0 else near[:-1]:
+                remote(
+                    v_o.at[sample, z_to * NY + y_places[d]],
+                    v_hin.at[k],
+                    bs_sem.at[sample],
+                    br_sem.at[0],
+                    {"sp_0": z_to, "sp_1": y_places[d], "dp": sample},
+                ).start()
+        if sample == 1:
+            v_hin[k] = v_o[1, k]
+
+    @pl.when(c == 1)
+    def _():
+        own_part(1)
+        own_part(0)
+
+    @pl.when(c == 0)
+    def _():
+        whole(v_o.at[0], v_hin, NSP, bs_sem.at[0], br_sem.at[0]).wait_recv()
+
+    @pl.when(c == 1)
+    def _():
+        whole(v_o.at[1], v_hin, NSP - 1, bs_sem.at[1], br_sem.at[0]).wait_recv()
+
     squares = jnp.zeros((TOK, 1), F32)
     gated = []
     for p in range(4):
@@ -513,10 +557,10 @@
         for s in range(2):
             h = 2 * p + s
             entering = v_hin[h * 8 : (h + 1) * 8].reshape(128, 128)
-            carried = dot(c_in, entering) * dot(growth, v_e[:, h * 128 : (h + 1) * 128])
+            carried = dot(c_in, entering) * v_g[h]
             sides.append(carried + pltpu.roll(carried, 64, 1))
         gate_in = v_f[3 + p // 2, 0:TOK, (p % 2) * 128 : (p % 2) * 128 + 128]
-        value = (v_y[p] + jnp.where(lane < 64, sides[0], sides[1])) * silu(gate_in)
+        value = (v_y[p] + jnp.where(lane < 64, sides[0], sides[1])) * gate_in
         squares = squares + jnp.sum(value * value, axis=-1, keepdims=True)
         gated.append(value)
     inv = lax.rsqrt(squares / 512.0 + EPS)
@@ -562,9 +606,17 @@
         for copy in first_copies:
             copy.wait_send()
 
-    ctx_wait.wait_send()
-    state_wait.wait_send()
-    back_wait.wait_send()
+    @pl.when(c == 0)
+    def _():
+        whole(v_cts, v_ctr.at[0], NSP, as_sem.at[0], ar_sem.at[0, 0]).wait_send()
+        whole(v_s, v_r.at[0], NSP, as_sem.at[1], ar_sem.at[1, 0]).wait_send()
+
+    @pl.when(c == 1)
+    def _():
+        whole(v_cts, v_ctr.at[1], NSP - 1, as_sem.at[0], ar_sem.at[0, 1]).wait_send()
+        whole(v_s, v_r.at[1], NSP - 1, as_sem.at[1], ar_sem.at[1, 1]).wait_send()
+        whole(v_o.at[0], v_hin, NSP, bs_sem.at[0], br_sem.at[0]).wait_send()
+        whole(v_o.at[1], v_hin, NSP - 1, bs_sem.at[1], br_sem.at[0]).wait_send()
 
 
 def shards(
@@ -617,13 +669,15 @@
         vmem((M, 128), F32),
         vmem((32, 1024), BF16),
         vmem((NSP, CTXR, 128), BF16),
-        vmem((NSP, CTXR, 128), BF16),
+        vmem((2, NSP, CTXR, 128), BF16),
         vmem((NSP, 16, 128), BF16),
-        vmem((NSP, 16, 128), BF16),
+        vmem((2, NSP, 16, 128), BF16),
         vmem((NSP, 8, 128), F32),
         vmem((NSP, 16, 128), F32),
+        vmem((2, NSP, 16, 128), BF16),
         vmem((NSP, 16, 128), BF16),
-        vmem((NSP, 16, 128), BF16),
+        vmem((4, TOK, 128), F32),
+        vmem((8, TOK, 128), F32),
         vmem((4, TOK, 128), F32),
         vmem((TOK, 512), BF16),
         vmem((2, TP, ROWS, 1024), BF16),
@@ -641,7 +695,10 @@
         dma((TP,)),
         dma((2, TP)),
         dma((2,)),
-        dma((6,)),
+        dma((2,)),
+        dma((2, 2)),
+        dma((2,)),
+        dma((1,)),
         dma((2, TP)),
         dma((2, TP)),
     ]

time: 54.2 us -> 52.7 us (0.972)
  Pallas kernels: 53.4 us -> 51.9 us
    pallas_call x1, Pallas kernels: 53.4 us -> 51.9 us  [shards(): call(latent, condition, context, context_source.reshape(16, 128), mod_wei...]
where the time goes in v3:
time: 52.7 us; the launch traced here: 52.6 us
  Pallas kernels  51.9 us (98%)
  local copies, waits for them, and re-layouts  0.66 us (1%)
    pallas_call x1, Pallas kernels, shards(): call(latent, condition, context, context_source.reshape(16, 128), mod_wei...  51.9 us

profile of v3, /device:TPU:8, one launch (start us, length us, event | category | flops | bytes accessed | tf_op | source)
XLA Modules:
  0.0 52.6 jit_solution(4365372773522360952)
XLA Ops:
  0.0 51.9 %mixer.1 = bf16[1,32,2048]{2,1,0:T(8,128)(2,1)S(1)} custom-call(bf16[1,32,2048]{2,1,0:T(8,128)(2,1)} %latent.1, bf16[1,2048]{1,0:T(2,128)(2,1)} %condition.1, bf16[1,8,2048]{2,1,0:T(8,128)(2,1)} %context.1, bf16[16,128]{1,0:T(8,128)(2,1)} %bitcast.5, bf16[3,32,512]{2,1,0:T(8,128)(2,1)} %mod_w.1, bf16[16,128]{1,0:T(8,128)(2,1)} %bitcast.6, ...), custom_call_target="tpu_custom_call" | custom-call | tf_op jit(solution)/shard_map/mixer/pallas_call | solution.py:716
  51.9 0.7 %copy.19 = bf16[1,32,2048]{2,1,0:T(8,128)(2,1)} copy(bf16[1,32,2048]{2,1,0:T(8,128)(2,1)S(1)} %mixer.1) | data formatting | bytes 262144

commit v4 on v3

--- a/solution.py
+++ b/solution.py
@@ -308,7 +308,7 @@
 
     for copy in z_copies:
         copy.wait_recv()
-    v_ms[...] = z_sum + sum(v_mz[d].astype(F32) for d in range(1, NZ))
+    v_ms[...] = (z_sum + sum(v_mz[d].astype(F32) for d in range(1, NZ))).astype(BF16)
     v_mx[t] = v_ms[...]
     x_copies = [
         remote(v_ms, v_mx.at[t], xs_sem.at[d], xr_sem.at[d], along_x(d)) for d in (2, 1, 3)
@@ -326,7 +326,7 @@
     gains = v_gain[...].astype(F32)
     for j in range(TP):
         cols = slice(j * 512, (j + 1) * 512)
-        mods = v_mx[j]
+        mods = v_mx[j].astype(F32)
         gain_j = jnp.concatenate([gains[4 * j + i : 4 * j + i + 1] for i in range(4)], axis=1)
         mul = gain_j * (1.0 + mods[1:2])
         add = mods[0:1]
@@ -368,21 +368,21 @@
     y_places = [lax.rem(y + d, NY) for d in range(NY)]
     near = (4, 3, 5, 2, 6, 1, 7, 0)
 
-    def to_owners(make, groups, src, dst, which):
-        for group in groups:
-            rows = [lax.rem(z + d, NZ) for d in group]
-            for h in rows:
-                make(h)
-            for d_z, h in zip(group, rows, strict=True):
-                for d in near if d_z else near[:-1]:
-                    remote(
-                        src.at[h * NY + y_places[d]],
-                        dst.at[c, k],
-                        as_sem.at[which],
-                        ar_sem.at[which, c],
-                        {"sp_0": h, "sp_1": y_places[d], "dp": 1},
-                    ).start()
-
+    def to_owners(make, group, src, dst, which):
+        rows = [lax.rem(z + d, NZ) for d in group]
+        for h in rows:
+            make(h)
+        for d_z, h in zip(group, rows, strict=True):
+            for d in near if d_z else near[:-1]:
+                remote(
+                    src.at[h * NY + y_places[d]],
+                    dst.at[c, k],
+                    as_sem.at[which],
+                    ar_sem.at[which, c],
+                    {"sp_0": h, "sp_1": y_places[d], "dp": 1},
+                ).start()
+
+    def to_own(src, dst, which):
         @pl.when(c == 0)
         def _():
             remote(src.at[k], dst.at[0, k], as_sem.at[which], ar_sem.at[which, 0], partner).start()
@@ -401,7 +401,7 @@
             tile = jnp.where(lane8 < 64, x_tile, jnp.where(lane8 < 80, b_tiles[n], tail))
             v_cts[h * 8 + n] = tile.astype(BF16)
 
-    to_owners(context_tiles, (near,), v_cts, v_ctr, 0)
+    to_owners(context_tiles, near[:4], v_cts, v_ctr, 0)
 
     has_before = jnp.where(k > 0, 1.0, 0.0)
     has_after = jnp.where(k < NSP - 1, 1.0, 0.0)
@@ -433,7 +433,11 @@
         for n in range(8):
             v_s[h * 8 + n] = state[n * 16 : (n + 1) * 16]
 
-    to_owners(state_tiles, (near[:4], near[4:]), v_s, v_r, 1)
+    to_owners(state_tiles, near[:4], v_s, v_r, 1)
+    to_owners(context_tiles, near[4:], v_cts, v_ctr, 0)
+    to_owners(state_tiles, near[4:], v_s, v_r, 1)
+    to_own(v_cts, v_ctr, 0)
+    to_own(v_s, v_r, 1)
 
     for i in (3, 4):
         v_f[i] = dot(v_h[...], v_w[i])
@@ -465,7 +469,24 @@
         v_f[3 + p // 2, 0:TOK, cols] = silu(v_f[3 + p // 2, 0:TOK, cols])
 
     row_c = iota((NSP * CTXR, 128), 0)
-    lane_c = iota((NSP * CTXR, 128), 1)
+    row16 = iota((16, 128), 0)
+    row_s = iota((16, NSP * CTXR), 0)
+
+    def one_hot(hits):
+        return jnp.where(hits, 1.0, 0.0).astype(BF16)
+
+    def turned(picks, values):
+        return lax.dot_general(picks, values, (((1,), (1,)), ((), ())), preferred_element_type=F32)
+
+    pick_steps = one_hot((row16 < 2) & (lane16 == 80 + 8 * row16 + z))
+    pick_b = one_hot(lane16 == 64 + row16)
+    side = 8 * lax.shift_right_logical(lane, 6) + z
+    pick_totals = one_hot((row == 96 + side) | (row == 112 + side))
+
+    def rate_of(at):
+        return jnp.sum(jnp.where(lane8[0:1] == at, rate, 0.0), axis=1, keepdims=True)
+
+    rate_c = jnp.where(row_s == 0, rate_of(z), jnp.where(row_s == 1, rate_of(z + 8), 0.0))
     x_lanes = pl.ds(pl.multiple_of((z // 2) * 128, 128), 128)
     x_shift = lax.rem(z, 2) * 64
     b_shift = lax.rem(192 - 16 * y, 128)
@@ -482,31 +503,26 @@
         down = jnp.where(row_c == 0, 0.0, pltpu.roll(feats, 1, 0))
         up = jnp.where(row_c == NSP * CTXR - 1, 0.0, pltpu.roll(feats, NSP * CTXR - 1, 0))
         smooth = silu(down * owner_tap(0) + feats * owner_tap(1) + up * owner_tap(2))
-        picked = pltpu.roll(feats, lax.rem(128 - z, 128), 1)
-        used = (lane_c == 80) | (lane_c == 88)
-        step_c = softplus(picked)
-        rate_c = pltpu.roll(jnp.broadcast_to(rate, (8, 128)), 80 - z, 1)[0:1]
-        decay_c = jnp.where(used, -rate_c * step_c, 0.0)
-        parts_c = high_low(decay_c, 1)
-        run = jnp.zeros((1, 128), F32)
+        smooth = smooth.astype(BF16)
+        feats = feats.astype(BF16)
+        step_c = softplus(turned(pick_steps, feats))
+        decay_c = -rate_c * step_c
+        high = decay_c.astype(BF16)
+        low = (decay_c - high.astype(F32)).astype(BF16)
+        run = jnp.zeros((16, 1), F32)
         pieces = []
         for b in range(4):
-            piece = dot(lower, parts_c[b * 128 : (b + 1) * 128]) + run
-            run = piece[127:128]
+            cols = slice(b * 128, (b + 1) * 128)
+            piece = dot(high[:, cols], upper) + dot(low[:, cols], upper) + run
+            run = piece[:, 127:128]
             pieces.append(piece)
-        prefix = jnp.concatenate(pieces, axis=0)
-        prefix = prefix + pltpu.roll(prefix, 127, 1)
-        end = prefix[NSP * CTXR - 1 :]
-        reach = jnp.where(lane_c < 84, end - prefix, prefix - decay_c)
-        weight_c = jnp.where(used, step_c * jnp.exp(jnp.where(used, reach, 0.0)), 0.0)
-        smooth = smooth.astype(BF16)
-        x_wide = smooth.astype(F32)
-        spread_x = jnp.where(
-            lane_c < 64, x_wide * weight_c[:, 80:81], pltpu.roll(x_wide, 64, 1) * weight_c[:, 88:89]
-        )
-        context_state = tdot(smooth, spread_x.astype(BF16))[64:80]
-        grow = jnp.exp(jnp.where((lane_c >= 96) & (lane_c < 112), picked + pltpu.roll(picked, 112, 1), 0.0))
-        v_dec[...] = jnp.where(lane_c < 64, grow[:, 96:97], grow[:, 104:105]).reshape(NSP, 8, 128)
+        prefix = jnp.concatenate(pieces, axis=1)
+        weight_c = step_c * jnp.exp(jnp.where(row_s == 0, run - prefix, prefix - decay_c))
+        b_turned_c = turned(pick_b, smooth)
+        both = jnp.concatenate([b_turned_c * weight_c[0:1], b_turned_c * weight_c[1:2]], axis=0)
+        both = dot(both.astype(BF16), smooth)
+        context_state = jnp.where(lane16 < 64, both[0:16], pltpu.roll(both[16:32], 64, 1))
+        v_dec[...] = jnp.exp(dot(feats, pick_totals)).reshape(NSP, 8, 128)
 
         whole(v_s, v_r.at[sample], count, as_sem.at[1], ar_sem.at[1, sample]).wait_recv()
 
@@ -591,7 +607,7 @@
             for d in range(1, TP):
                 mixed = mixed + v_pr[n, d, :, cols].astype(F32)
             j = n * 2 + q
-            out[0, :, j * 512 : (j + 1) * 512] = (v_mx[j, 2:3] * mixed).astype(BF16)
+            out[0, :, j * 512 : (j + 1) * 512] = (v_mx[j].astype(F32)[2:3] * mixed).astype(BF16)
 
     for copy in y_copies + z_copies + x_copies + lat_copies + w_copies + out_copies:
         copy.wait_send()
@@ -660,8 +676,8 @@
         vmem((NY, 8, 512), BF16),
         vmem((8, 512), BF16),
         vmem((NZ, 8, 512), BF16),
-        vmem((8, 512), F32),
-        vmem((TP, 8, 512), F32),
+        vmem((8, 512), BF16),
+        vmem((TP, 8, 512), BF16),
         vmem((2, 1, D), F32),
         vmem((2, 1, D), F32),
         vmem((M, D), BF16),

time: 52.7 us -> 52.8 us (level)
  no operation moved by 1% of the time
where the time goes in v4:
time: 52.8 us; the launch traced here: 52.7 us
  Pallas kernels  52 us (98%)
  local copies, waits for them, and re-layouts  0.66 us (1%)
    pallas_call x1, Pallas kernels, shards(): call(latent, condition, context, context_source.reshape(16, 128), mod_wei...  52 us

profile of v4, /device:TPU:8, one launch (start us, length us, event | category | flops | bytes accessed | tf_op | source)
XLA Modules:
  0.0 52.7 jit_solution(17749142360380180897)
XLA Ops:
  0.0 52.0 %mixer.1 = bf16[1,32,2048]{2,1,0:T(8,128)(2,1)S(1)} custom-call(bf16[1,32,2048]{2,1,0:T(8,128)(2,1)} %latent.1, bf16[1,2048]{1,0:T(2,128)(2,1)} %condition.1, bf16[1,8,2048]{2,1,0:T(8,128)(2,1)} %context.1, bf16[16,128]{1,0:T(8,128)(2,1)} %bitcast.5, bf16[3,32,512]{2,1,0:T(8,128)(2,1)} %mod_w.1, bf16[16,128]{1,0:T(8,128)(2,1)} %bitcast.6, ...), custom_call_target="tpu_custom_call" | custom-call | tf_op jit(solution)/shard_map/mixer/pallas_call | solution.py:732
  52.0 0.7 %copy.19 = bf16[1,32,2048]{2,1,0:T(8,128)(2,1)} copy(bf16[1,32,2048]{2,1,0:T(8,128)(2,1)S(1)} %mixer.1) | data formatting | bytes 262144
